TPU v7x, 256 devices: a whole 4x4x8 slice. The times are simulated.
256 devices in a mesh: sp: 32 (over z, x), tp: 8 (over y, core).
Axes of the slice: x: 4, y: 4, z: 8, core: 2. Of those that a mesh axis runs over, the one named last changes fastest.
Arguments:
- residual: bfloat16 [10240, 2048], P(('sp', 'tp')), may hold values from -6 to 6
- query_narrow: bfloat16 [10240, 1024], P('sp', 'tp'), may hold values from -48 to 48
- key_narrow: bfloat16 [10240, 1024], P('sp', 'tp'), may hold values from -48 to 48
- value_narrow: bfloat16 [10240, 1024], P('sp', 'tp'), may hold values from -6 to 6
- query_wide: bfloat16 [10240, 2048], P('sp', 'tp'), may hold values from -48 to 48
- key_wide: bfloat16 [10240, 2048], P('sp', 'tp'), may hold values from -48 to 48
- value_wide: bfloat16 [10240, 1024], P('sp', 'tp'), may hold values from -6 to 6
- subtract_narrow: float32 [8], P('tp'), may hold values from 0.3 to 0.8
- subtract_wide: float32 [8], P('tp'), may hold values from 0.3 to 0.8
- head_gain: float32 [128], replicated, may hold values from 0.1 to 1.9
- out_narrow: bfloat16 [1024, 2048], replicated, may hold values from -0.125 to 0.125
- out_wide: bfloat16 [1024, 2048], replicated, may hold values from -0.125 to 0.125
- norm1_gain: float32 [2048], replicated, may hold values from 0.1 to 1.9
- norm2_gain: float32 [2048], replicated, may hold values from 0.1 to 1.9
- expert_ids: int32 [10240, 2], P(('sp', 'tp')), may hold values from 0 to 31, all different within a row; in each aligned block of 40 rows (0 to 39, 40 to 79, ...) at most 3 rows name the same one
- expert_weight: float32 [10240, 2], P(('sp', 'tp')), may hold values from 0.1 to 1
- gate_proj: bfloat16 [32, 2048, 2048], P('sp', None, 'tp'), may hold values from -0.125 to 0.125
- up_proj: bfloat16 [32, 2048, 2048], P('sp', None, 'tp'), may hold values from -0.125 to 0.125
- down_proj: bfloat16 [32, 2048, 2048], P('sp', 'tp'), may hold values from -0.125 to 0.125
Outputs:
- layer_out: bfloat16 [10240, 2048], P(('sp', 'tp'))
Inputs may be any that keep to these rules, and one draw needn't show every extreme that they name: `expert_ids`: each row names 2 different experts. Among the 40 rows of one device no expert is named more than 3 times, and in some device's rows some expert is named exactly 3 times.
All inputs are finite; a program needn't handle non-finite values.
Results may differ from a plain program's by a relative error of at most 0.014.
Values may be sent and summed in bfloat16 or wider, within the bound.
A program may use at most 128 MiB of HBM per device.

v0:
```python
import jax
import jax.numpy as jnp
from jax import lax
from jax.sharding import PartitionSpec as P

residual_scale = 2.0**0.5


def in_one_piece(arrays, axis, dim, along):
    ends, at = ([], 0)
    for a in arrays[:-1]:
        at += a.shape[along]
        ends.append(at)
    both = jnp.concatenate(arrays, axis=along)
    return tuple(jnp.split(lax.all_gather(both, axis, axis=dim, tiled=True), ends, axis=along))


def in_blocks(value, dim, devices):
    before, after = (value.shape[:dim], value.shape[dim + 1 :])
    return jnp.moveaxis(value.reshape(*before, devices, -1, *after), dim, 0)


def sent_and_summed(value, axis, dim):
    devices = lax.axis_size(axis)
    pieces = lax.all_to_all(in_blocks(value, dim, devices), axis, 0, 0, tiled=True)
    return jnp.sum(pieces.astype(jnp.float32), axis=0)


def items_in_groups(value, axis, split_dim, concat_dim, work, item_dim, out_dim):
    items = jax.tree.leaves(value)[0].shape[item_dim]
    count = 2 if items % 2 == 0 else 1
    outs = []
    for k in range(count):
        group = jax.tree.map(
            lambda a: lax.slice_in_dim(
                a, k * (items // count), (k + 1) * (items // count), axis=item_dim
            ),
            value,
        )
        outs.append(
            work(
                lax.all_to_all(
                    group, axis, split_axis=split_dim, concat_axis=concat_dim, tiled=True
                )
            )
        )
    return jax.tree.map(lambda *parts: jnp.concatenate(parts, axis=out_dim), *outs)


def layer_norm(values, gain):
    center = jnp.mean(values, -1, keepdims=True)
    spread = jnp.mean(jnp.square(values - center), -1, keepdims=True)
    return (values - center) * lax.rsqrt(spread + 1e-05) * gain


def block_take(shards, shard_rows):
    take = shards
    for count in range(shards, 0, -1):
        if shards % count == 0 and count * shard_rows >= 512:
            take = count
    return take


def start_carry(head_count, tok_rows, value_size):
    return (
        jnp.full((head_count, 2, tok_rows), -1e30, jnp.float32),
        jnp.zeros((head_count, 2, tok_rows), jnp.float32),
        jnp.zeros((head_count, 2, tok_rows, value_size), jnp.float32),
    )


def absorb_keys(carry, queries, key_piece, value_piece, shard_rows):
    head_count = queries.shape[1]
    key_size = queries.shape[3]
    shards = key_piece.shape[0] // shard_rows
    take = block_take(shards, shard_rows)
    span = take * shard_rows

    def one_block(step_index, state):
        rowtop, total, summed = state
        key_block = lax.dynamic_slice_in_dim(key_piece, step_index * span, span, 0).reshape(
            span, head_count, 2, key_size
        )
        value_block = lax.dynamic_slice_in_dim(value_piece, step_index * span, span, 0).reshape(
            span, head_count, -1
        )
        scores = jnp.einsum(
            "qhmd,khmd->hmqk", queries, key_block, preferred_element_type=jnp.float32
        ) * key_size ** (-0.5)
        newtop = jnp.maximum(rowtop, jnp.max(scores, -1))
        shrink = jnp.exp(rowtop - newtop)
        expo = jnp.exp(scores - newtop[..., None])
        total = total * shrink + jnp.sum(expo, -1)
        summed = summed * shrink[..., None] + jnp.einsum(
            "hmqk,khe->hmqe",
            expo.astype(jnp.bfloat16),
            value_block,
            preferred_element_type=jnp.float32,
        )
        return (newtop, total, summed)

    return lax.fori_loop(0, shards // take, one_block, carry)


def finish_heads(carry, subtract, head_gain):
    rowtop, total, summed = carry
    mapped = summed / total[..., None]
    diff = mapped[:, 0] - subtract[:, None, None] * mapped[:, 1]
    normed = diff * lax.rsqrt(jnp.mean(diff * diff, -1, keepdims=True) + 1e-06) * head_gain
    return jnp.transpose(normed, (1, 0, 2)).reshape(diff.shape[1], -1).astype(jnp.bfloat16)


def on_device(
    residual,
    query_narrow,
    key_narrow,
    value_narrow,
    query_wide,
    key_wide,
    value_wide,
    subtract_narrow,
    subtract_wide,
    head_gain,
    out_narrow,
    out_wide,
    norm1_gain,
    norm2_gain,
    expert_ids,
    expert_weight,
    gate_proj,
    up_proj,
    down_proj,
):
    tok_rows = query_narrow.shape[0]
    head_count = subtract_narrow.shape[0]
    value_size = head_gain.shape[0]
    narrow_queries = query_narrow.reshape(tok_rows, head_count, 2, -1)
    wide_queries = query_wide.reshape(tok_rows, head_count, 2, -1)
    narrow_start = start_carry(head_count, tok_rows, value_size)
    wide_start = start_carry(head_count, tok_rows, value_size)
    pieces = in_one_piece((key_narrow, value_narrow), "sp", 0, 1)
    narrow_state = absorb_keys(narrow_start, narrow_queries, pieces[0], pieces[1], tok_rows)
    pieces = in_one_piece((key_wide, value_wide), "sp", 0, 1)
    wide_state = absorb_keys(wide_start, wide_queries, pieces[0], pieces[1], tok_rows)
    attended_narrow = finish_heads(narrow_state, subtract_narrow, head_gain)
    attended_wide = finish_heads(wide_state, subtract_wide, head_gain)
    offset = lax.axis_index("tp") * head_count * value_size
    local_narrow = lax.dynamic_slice_in_dim(out_narrow, offset, head_count * value_size, 0)
    local_wide = lax.dynamic_slice_in_dim(out_wide, offset, head_count * value_size, 0)
    mix = sent_and_summed(
        (
            jnp.dot(attended_narrow, local_narrow, preferred_element_type=jnp.float32)
            + jnp.dot(attended_wide, local_wide, preferred_element_type=jnp.float32)
        ).astype(jnp.bfloat16),
        "tp",
        0,
    )
    hidden = layer_norm(residual_scale * residual.astype(jnp.float32) + mix, norm1_gain).astype(
        jnp.bfloat16
    )
    local_rows, top_count = expert_ids.shape
    experts = lax.axis_size("sp")
    capacity = max(2, 3 * local_rows * top_count // (2 * experts))
    flat_ids = expert_ids.reshape(-1)
    onehot = (flat_ids[:, None] == jnp.arange(experts, dtype=jnp.int32)[None, :]).astype(jnp.int32)
    before = jnp.cumsum(onehot, 0) - onehot
    position = jnp.sum(before * onehot, 1)
    slots = (flat_ids * capacity + position).reshape(local_rows, top_count)
    dispatch_table = jnp.any(
        jnp.arange(experts * capacity, dtype=jnp.int32)[:, None, None] == slots[None], -1
    ).astype(jnp.bfloat16)
    outgoing = jnp.dot(dispatch_table, hidden, preferred_element_type=jnp.float32).astype(
        jnp.bfloat16
    )
    outgoing = outgoing.reshape(experts, capacity, -1)

    def run_expert(received):
        gathered = lax.all_gather(received, "tp", axis=1, tiled=True)
        flat_rows = gathered.reshape(-1, gathered.shape[2])
        gate_part = jnp.dot(flat_rows, gate_proj[0], preferred_element_type=jnp.float32)
        up_part = jnp.dot(flat_rows, up_proj[0], preferred_element_type=jnp.float32)
        inner = (jax.nn.silu(gate_part) * up_part).astype(jnp.bfloat16)
        partial_out = jnp.dot(inner, down_proj[0], preferred_element_type=jnp.float32).reshape(
            gathered.shape
        )
        summed = lax.psum_scatter(
            partial_out.astype(jnp.bfloat16), "tp", scatter_dimension=1, tiled=True
        )
        return lax.all_to_all(summed, "sp", split_axis=0, concat_axis=0, tiled=True)

    returned = items_in_groups(outgoing, "sp", 0, 0, run_expert, 1, 1)
    returned_flat = returned.reshape(experts * capacity, -1)
    picked = returned_flat[slots].astype(jnp.float32)
    routed = jnp.sum(expert_weight[..., None] * picked, 1)
    return layer_norm(residual_scale * hidden.astype(jnp.float32) + routed, norm2_gain).astype(
        jnp.bfloat16
    )


def solution(mesh):
    placed = (
        P(("sp", "tp"), None),
        P("sp", "tp"),
        P("sp", "tp"),
        P("sp", "tp"),
        P("sp", "tp"),
        P("sp", "tp"),
        P("sp", "tp"),
        P("tp"),
        P("tp"),
        P(),
        P(),
        P(),
        P(),
        P(),
        P(("sp", "tp"), None),
        P(("sp", "tp"), None),
        P("sp", None, "tp"),
        P("sp", None, "tp"),
        P("sp", "tp", None),
    )
    return jax.shard_map(
        on_device, mesh=mesh, in_specs=placed, out_specs=P(("sp", "tp"), None), check_vma=False
    )
```

profile of v0, /device:TPU:2, one launch (start us, length us, event | category | flops | bytes accessed | tf_op | source)
XLA Modules:
  0.0 421.5 jit_solution(8756736317949425885)
XLA Ops:
  6.5 1.7 pad_maximum_fusion.1
  8.3 1.7 pad_maximum_fusion
  10.1 1.6 copy.88
  14.7 81.8 %all-gather.4.cloned.1.call-done = bf16[10240,256]{1,0:T(8,128)(2,1)} async-done(((bf16[320,256]{1,0:T(8,128)(2,1)}), bf16[10240,256]{1,0:T(8,128)(2,1)}) %all-gather.4.cloned.1.call-update) | async-done | bytes 5242896 | tf_op jit(solution)/shard_map/all_gather | solution.py:15
  96.5 4.1 fusion.57
  100.7 71.9 %while.36 = (s32[]{:T(128)}, f32[1,2,320]{2,1,0:T(2,128)S(1)}, f32[1,2,320]{2,1,0:T(2,128)S(1)}, f32[1,2,320,128]{3,2,1,0:T(8,128)S(1)}, bf16[10240,128]{1,0:T(8...) while((s32[]{:T(128)}, f32[1,2,320]{2,1,0:T(2,128)S(1)}, ...), condition=%wide.region_3.0_spmd.clone, body=%wide.region_0.0_spmd.clone.sunk | while | flops 160812800 | bytes 6676655 | solution.py:102
  103.2 1.4 fusion.82
  107.7 1.5 fusion.82
  112.2 1.4 fusion.82
  116.7 1.4 fusion.82
  121.2 1.4 fusion.82
  125.7 1.5 fusion.82
  130.2 1.5 fusion.82
  134.7 1.4 fusion.82
  139.2 1.5 fusion.82
  143.7 1.5 fusion.82
  148.1 1.5 fusion.82
  152.7 1.4 fusion.82
  157.2 1.4 fusion.82
  161.6 1.5 fusion.82
  166.1 1.4 fusion.82
  170.6 1.5 fusion.82
  172.9 3.1 fusion.35
  176.0 15.4 %all-gather.6.cloned.1.call-done = bf16[10240,384]{1,0:T(8,128)(2,1)} async-done(((bf16[320,384]{1,0:T(8,128)(2,1)}), bf16[10240,384]{1,0:T(8,128)(2,1)}) %all-gather.6.cloned.1.call-update) | async-done | bytes 7864336 | tf_op jit(solution)/shard_map/all_gather | solution.py:15
  191.4 4.2 split.18
  195.6 2.9 split.19
  198.5 58.4 %while.37 = (s32[]{:T(128)}, f32[1,2,320]{2,1,0:T(2,128)S(1)}, f32[1,2,320]{2,1,0:T(2,128)S(1)}, f32[1,2,320,128]{3,2,1,0:T(8,128)S(1)}, bf16[10240,256]{1,0:T(8...) while((s32[]{:T(128)}, f32[1,2,320]{2,1,0:T(2,128)S(1)}, ...), condition=%wide.region_8.0_spmd.clone, body=%wide.region_5.8_spmd.clone.sunk | while | flops 213241600 | bytes 7577775 | solution.py:102
  200.2 1.4 fusion.88
  203.8 1.4 fusion.88
  207.5 1.4 fusion.88
  214.8 1.4 fusion.88
  222.1 1.4 fusion.88
  229.4 1.4 fusion.88
  236.7 1.4 fusion.88
  244.0 1.4 fusion.88
  251.3 1.4 fusion.88
  257.2 3.5 fusion.28
  260.8 4.4 %all-to-all-start = ((bf16[8,40,2048]{2,1,0:T(8,128)(2,1)}), bf16[8,40,2048]{2,1,0:T(8,128)(2,1)S(1)}, u32[]{:S(2)}, u32[]{:S(2)}) async-start(bf16[8,40,2048]{2,1,0:T(8,128)(2,1)} %bitcast.7), calls=%async_computation | async-start | bytes 2621440 | tf_op jit(solution)/shard_map/all_to_all | solution.py:25
  266.1 17.8 %all-to-all-done = bf16[8,40,2048]{2,1,0:T(8,128)(2,1)S(1)} async-done(((bf16[8,40,2048]{2,1,0:T(8,128)(2,1)}), bf16[8,40,2048]{2,1,0:T(8,128)(2,1)S(1)}, u32[]{:S(2)}, u32[]{:S(2)}) %all-to-all-start) | async-done | bytes 1310752 | tf_op jit(solution)/shard_map/all_to_all | solution.py:25
  285.2 23.5 %all_to_all.15 = bf16[32,3,2048]{2,1,0:T(4,128)(2,1)S(1)} all-to-all(bf16[32,3,2048]{2,1,0:T(4,128)(2,1)S(1)} %reshape.302), channel_id=1, replica_groups=mesh['sp'=32,'tp'=8] {'sp'}, dimensions={0} | all-to-all | bytes 786432 | tf_op jit(solution)/shard_map/all_to_all | solution.py:42
  310.0 25.1 %all-gather.8.cloned.1.call-done = bf16[32,24,2048]{2,0,1:T(8,128)(2,1)} async-done(((bf16[32,3,2048]{2,0,1:T(8,128)(2,1)}), bf16[32,24,2048]{2,0,1:T(8,128)(2,1)}) %all-gather.8.cloned.1.call-update) | async-done | bytes 3145744 | tf_op jit(solution)/shard_map/all_gather | solution.py:178
  335.1 3.6 copy.96
  338.7 2.3 fusion.32
  343.0 3.4 copy.97
  346.4 38.6 %reduce-scatter.2.cloned.1.call-done = bf16[32,3,2048]{2,0,1:T(8,128)(2,1)} async-done(((bf16[32,24,2048]{2,0,1:T(8,128)(2,1)}), bf16[32,3,2048]{2,0,1:T(8,128)(2,1)}) %reduce-scatter.2.cloned.1.call-update) | async-done | bytes 393232 | tf_op jit(solution)/shard_map/reduce_scatter | solution.py:186
  385.1 2.1 copy.98
  387.2 10.1 %all-to-all-start.2 = ((bf16[32,3,2048]{2,1,0:T(4,128)(2,1)}), bf16[32,3,2048]{2,1,0:T(4,128)(2,1)S(1)}, u32[]{:S(2)}, u32[]{:S(2)}) async-start(bf16[32,3,2048]{2,1,0:T(4,128)(2,1)} %copy.98), calls=%async_computation.3 | async-start | bytes 1048576 | tf_op jit(solution)/shard_map/all_to_all | solution.py:189
  397.6 13.6 %all-to-all-done.2 = bf16[32,3,2048]{2,1,0:T(4,128)(2,1)S(1)} async-done(((bf16[32,3,2048]{2,1,0:T(4,128)(2,1)}), bf16[32,3,2048]{2,1,0:T(4,128)(2,1)S(1)}, u32[]{:S(2)}, u32[]{:S(2)}) %all-to-all-start.2) | async-done | bytes 393248 | tf_op jit(solution)/shard_map/all_to_all | solution.py:189
  (304 shorter events, 104.1 us)
Async XLA Ops:
  6.5 335.5 %copy-start = (bf16[1,256,2048]{2,1,0:T(8,128)(2,1)S(1)}, bf16[1,256,2048]{2,1,0:T(8,128)(2,1)}, u32[]{:S(2)}) copy-start(bf16[1,256,2048]{2,1,0:T(8,128)(2,1)} %param.41) | copy-start | bytes 3145732
  6.5 90.0 %all-gather.4.cloned.1.call-start = ((), (), s32[]{:S(2)}) async-start(), calls=%async_computation.4 | async-start | bytes 5406720 | tf_op jit(solution)/shard_map/all_gather | solution.py:15
  8.3 183.1 %all-gather.6.cloned.1.call-start = ((), (), s32[]{:S(2)}) async-start(), calls=%async_computation.5 | async-start | bytes 8110080 | tf_op jit(solution)/shard_map/all_gather | solution.py:15
  100.7 72.3 %copy-start.6 = (f32[128]{0:T(128)S(1)}, f32[128]{0:T(128)}, u32[]{:S(2)}) copy-start(f32[128]{0:T(128)} %param.32) | copy-start | bytes 1540
  195.6 2.9 copy-start.1
  257.2 8.0 %copy-start.5 = (s32[40,2]{0,1:T(2,128)S(1)}, s32[40,2]{0,1:T(2,128)}, u32[]{:S(2)}) copy-start(s32[40,2]{0,1:T(2,128)} %param.37) | copy-start | bytes 964
  260.8 23.4 %copy-start.2 = (bf16[40,2048]{1,0:T(8,128)(2,1)S(1)}, bf16[40,2048]{1,0:T(8,128)(2,1)}, u32[]{:S(2)}) copy-start(bf16[40,2048]{1,0:T(8,128)(2,1)} %param.23) | copy-start | bytes 491524
  260.8 23.8 %copy-start.3 = (f32[2048]{0:T(1024)S(1)}, f32[2048]{0:T(1024)}, u32[]{:S(2)}) copy-start(f32[2048]{0:T(1024)} %param.35) | copy-start | bytes 24580
  260.8 23.2 %all-to-all-start = ((bf16[8,40,2048]{2,1,0:T(8,128)(2,1)}), bf16[8,40,2048]{2,1,0:T(8,128)(2,1)S(1)}, u32[]{:S(2)}, u32[]{:S(2)}) async-start(bf16[8,40,2048]{2,1,0:T(8,128)(2,1)} %bitcast.7), calls=%async_computation | async-start | bytes 2621440 | tf_op jit(solution)/shard_map/all_to_all | solution.py:25
  265.2 69.9 %all-gather.8.cloned.1.call-start = ((), (), s32[]{:S(2)}) async-start(), calls=%async_computation.6 | async-start | bytes 3538944 | tf_op jit(solution)/shard_map/all_gather | solution.py:178
  309.8 75.3 %reduce-scatter.2.cloned.1.call-start = ((), (), s32[]{:S(2)}) async-start(), calls=%async_computation.7 | async-start | bytes 3538944 | tf_op jit(solution)/shard_map/reduce_scatter | solution.py:186
  338.7 2.3 copy-start.8
  346.4 51.1 %copy-start.7 = (f32[40,2]{0,1:T(2,128)S(1)}, f32[40,2]{0,1:T(2,128)}, u32[]{:S(2)}) copy-start(f32[40,2]{0,1:T(2,128)} %param.38) | copy-start | bytes 964
  387.2 24.0 %all-to-all-start.2 = ((bf16[32,3,2048]{2,1,0:T(4,128)(2,1)}), bf16[32,3,2048]{2,1,0:T(4,128)(2,1)S(1)}, u32[]{:S(2)}, u32[]{:S(2)}) async-start(bf16[32,3,2048]{2,1,0:T(4,128)(2,1)} %copy.98), calls=%async_computation.3 | async-start | bytes 1048576 | tf_op jit(solution)/shard_map/all_to_all | solution.py:189
  411.6 2.6 copy-start.4
Sparse Core Ops, SparseCore 0:
  9.9 86.5 all-gather.3
  99.1 92.2 all-gather.5
  309.9 25.1 all-gather.7
  346.6 38.4 reduce-scatter.1
where the time goes:
time: 425 us; the launch traced here: 421 us
  waiting for transfers between devices  192 us (45%)
  matrix products  87.6 us (21%)
  local copies, waits for them, and re-layouts  64.1 us (15%)
  blocking collectives  23.5 us (6%)
  other arithmetic  22.6 us (5%)
  starting transfers between devices  14.8 us (3%)
  between operations  14.7 us (3%)
    all_gather x2, waiting for transfers between devices, in_one_piece(): lax.all_gather(both, axis, axis=dim, tiled=True)  97.2 us
    dot_general x32, matrix products, one_block(): jnp.einsum('hmqk,khe->hmqe', expo.astype(jnp.bfloat16), value_block, pref...  46.3 us
    reduce_scatter x1, waiting for transfers between devices, run_expert(): lax.psum_scatter(partial_out.astype(jnp.bfloat16), 'tp', scatter_dimensio...  38.6 us
    dynamic_slice x64, local copies, waits for them, and re-layouts, one_block(): lax.dynamic_slice_in_dim(key_piece, step_index * span, span, 0)  36.8 us
    dot_general x32, matrix products, one_block(): jnp.einsum('qhmd,khmd->hmqk', queries, key_block, preferred_element_type=...  30.2 us
    all_gather x1, waiting for transfers between devices, run_expert(): gathered = lax.all_gather(received, 'tp', axis=1, tiled=True)  25.1 us
    all_to_all x1, blocking collectives, items_in_groups(): lax.all_to_all(group, axis, split_axis=split_dim, concat_axis=concat_dim,...  23.5 us
    all_to_all x1, waiting for transfers between devices, sent_and_summed(): lax.all_to_all(in_blocks(value, dim, devices), axis, 0, 0, tiled=True)  17.8 us
  transfers between devices with their start and end apart: 6, of which 6 were waited for; matrix products, arithmetic and copies ran while one was open for 20% of the time, Pallas kernels for 0%

commit v1 on v0

v1 whole, which is shorter than its diff:
```python
import functools

import jax
import jax.numpy as jnp
from jax import lax
from jax.experimental import pallas as pl
from jax.experimental.pallas import tpu as pltpu
from jax.sharding import PartitionSpec as P

residual_scale = 2.0**0.5
MESH = pl.DeviceIdType.MESH


def items_in_groups(value, axis, split_dim, concat_dim, work, item_dim, out_dim):
    items = jax.tree.leaves(value)[0].shape[item_dim]
    count = 2 if items % 2 == 0 else 1
    outs = []
    for k in range(count):
        group = jax.tree.map(
            lambda a: lax.slice_in_dim(
                a, k * (items // count), (k + 1) * (items // count), axis=item_dim
            ),
            value,
        )
        outs.append(
            work(
                lax.all_to_all(
                    group, axis, split_axis=split_dim, concat_axis=concat_dim, tiled=True
                )
            )
        )
    return jax.tree.map(lambda *parts: jnp.concatenate(parts, axis=out_dim), *outs)


def layer_norm(values, gain):
    center = jnp.mean(values, -1, keepdims=True)
    spread = jnp.mean(jnp.square(values - center), -1, keepdims=True)
    return (values - center) * lax.rsqrt(spread + 1e-05) * gain


LOG2E = 1.4426950408889634
Z_RING = 8
X_RING = 4
NARROW = (128, 384)
WIDE = (384, 768)
ROW = 896
PLACE = (0, 1, 3, 5, 7, 6, 4, 2)
QPLACE = (3, 1, 0, 2)


def attend_kernel(
    tok,
    query_narrow,
    key_narrow,
    value_narrow,
    query_wide,
    key_wide,
    value_wide,
    subtract,
    head_gain,
    out,
    queries,
    keys,
    top,
    acc,
    stats,
    share,
    share_stats,
    got,
    got_stats,
    attended,
    gathered,
    local_sem,
    q_send,
    q_recv,
    kv_send,
    kv_recv,
    o_send,
    o_recv,
    s_send,
    s_recv,
    a_send,
    a_recv,
):
    sp = lax.axis_index("sp")
    tp = lax.axis_index("tp")
    heads = lax.axis_size("tp")
    z, x = sp // X_RING, sp % X_RING

    def along_z(k):
        return (lax.rem(z + k, Z_RING) * X_RING + x, tp)

    def along_x(k):
        return (z * X_RING + lax.rem(x + k, X_RING), tp)

    def along_tp(k):
        return (sp, lax.rem(tp + k, heads))

    own_q = QPLACE[0] * tok
    loads = [
        pltpu.make_async_copy(src, dst, local_sem.at[i])
        for i, (src, dst) in enumerate(
            (
                (query_narrow, queries.at[pl.ds(own_q, tok), pl.ds(0, 128)]),
                (query_wide, queries.at[pl.ds(own_q, tok), pl.ds(128, 256)]),
                (value_narrow, keys.at[pl.ds(0, tok), pl.ds(128, 128)]),
                (key_narrow, keys.at[pl.ds(0, tok), pl.ds(256, 128)]),
                (key_wide, keys.at[pl.ds(0, tok), pl.ds(384, 256)]),
                (value_wide, keys.at[pl.ds(0, tok), pl.ds(640, 128)]),
            )
        )
    ]
    for c in loads:
        c.start()

    barrier = pltpu.get_barrier_semaphore()
    peers = (
        [along_z(1), along_z(Z_RING - 1)]
        + [along_x(k) for k in range(1, X_RING)]
        + [along_tp(k) for k in range(1, heads)]
    )
    for peer in peers:
        pl.semaphore_signal(barrier, inc=1, device_id=peer, device_id_type=MESH)
    keys[:, 0:128] = jnp.ones((keys.shape[0], 128), jnp.bfloat16)
    keys[:, 768:896] = jnp.ones((keys.shape[0], 128), jnp.bfloat16)
    top[...] = jnp.full(top.shape, -1e30, jnp.float32)
    acc[...] = jnp.zeros(acc.shape, jnp.float32)
    stats[...] = jnp.zeros(stats.shape, jnp.float32)
    for c in loads:
        c.wait()
    pl.semaphore_wait(barrier, len(peers))

    def remote(src, dst, send, recv, peer):
        return pltpu.make_async_remote_copy(
            src_ref=src, dst_ref=dst, send_sem=send, recv_sem=recv, device_id=peer,
            device_id_type=MESH,
        )

    def ring_copy(way, step, piece):
        cols = WIDE if piece else NARROW
        forward = way == 0
        source = (Z_RING - step + 1) % Z_RING if forward else step - 1
        target = (Z_RING - step) % Z_RING if forward else step
        r0, rows = 0, tok
        if 2 * step == Z_RING:
            rows = tok // 2
            r0 = 0 if forward else rows
        at = lambda k: keys.at[
            pl.ds(PLACE[k] * tok + r0, rows), pl.ds(cols[0], cols[1] - cols[0])
        ]
        n = (way * (Z_RING // 2) + step - 1) * 2 + piece
        return remote(
            at(source), at(target), kv_send.at[n], kv_recv.at[n],
            along_z(1 if forward else Z_RING - 1),
        )

    def query_copy(k):
        return remote(
            queries.at[pl.ds(own_q, tok), :],
            queries.at[pl.ds(QPLACE[(X_RING - k) % X_RING] * tok, tok), :],
            q_send.at[k], q_recv.at[k], along_x(k),
        )

    ring = {
        (w, s, p): ring_copy(w, s, p)
        for w in range(2)
        for s in range(1, Z_RING // 2 + 1)
        for p in range(2)
    }
    query_copies = {k: query_copy(k) for k in range(1, X_RING)}

    def start_step(step, piece):
        for w in range(2):
            ring[w, step, piece].start()

    def arrived(step, piece):
        for w in range(2):
            ring[w, step, piece].wait_recv()

    start_step(1, 0)
    for k in (1, 3, 2):
        query_copies[k].start()
    start_step(1, 1)

    pair = 2 * tok

    def absorb(head, group, k0, span):
        rows = pl.ds(k0, span)
        qrows = pl.ds(group * pair, pair)
        size = 128 if head else 64
        scale = size**-0.5 * LOG2E
        scores = []
        for m in range(2):
            if head:
                q = queries[qrows, 128 + 128 * m : 256 + 128 * m]
                k = keys[rows, 384 + 128 * m : 512 + 128 * m]
            else:
                q = queries[qrows, 0:128]
                lane = lax.broadcasted_iota(jnp.int32, q.shape, 1)
                q = jnp.where((lane < 64) if m == 0 else (lane >= 64), q, jnp.zeros_like(q))
                k = keys[rows, 256:384]
            scores.append(
                lax.dot_general(
                    q, k, (((1,), (1,)), ((), ())), preferred_element_type=jnp.float32
                )
            )
        v = keys[rows, 640:896] if head else keys[rows, 0:256]
        for m in range(2):
            s = scores[m]
            before = top[2 * head + m, qrows, :]
            now = jnp.maximum(before, jnp.max(s, -1, keepdims=True) * scale)
            expo = jnp.exp2(s * scale - now[:, :1])
            shrink = jnp.exp2(before - now)
            add = jnp.dot(expo.astype(jnp.bfloat16), v, preferred_element_type=jnp.float32)
            a = acc[2 * head + m, qrows, :]
            acc[2 * head + m, qrows, :] = (
                jnp.concatenate([a[:, :128] * shrink, a[:, 128:] * shrink], 1) + add
            )
            top[2 * head + m, qrows, :] = now

    def absorb_both(head, k0, span):
        def one(g, carry):
            absorb(head, g, k0, span)
            return carry

        lax.fori_loop(0, 2, one, 0)

    def share_copy(head, k):
        to = (X_RING - k) % X_RING
        n = head * X_RING + k
        return (
            remote(share.at[n], got.at[head * X_RING + to], o_send.at[n], o_recv.at[n], along_x(k)),
            remote(
                share_stats.at[n], got_stats.at[head * X_RING + to], s_send.at[n], s_recv.at[n],
                along_x(k),
            ),
        )

    def finish(head, k):
        n = head * X_RING + k
        qrows = pl.ds(QPLACE[k] * tok, tok)
        lane = lax.broadcasted_iota(jnp.int32, (tok, 128), 1)
        column = jnp.zeros((tok, 128), jnp.float32)
        parts = []
        for m in range(2):
            a = acc[2 * head + m, qrows, :]
            value, total = (a[:, :128], a[:, 128:]) if head else (a[:, 128:], a[:, :128])
            parts.append(value / total)
            column = jnp.where(lane == m, top[2 * head + m, qrows, :] + jnp.log2(total), column)
        both = jnp.concatenate(parts, 1)
        if k == 0:
            got[n] = both.astype(jnp.bfloat16)
        else:
            share[n] = both.astype(jnp.bfloat16)
        stats[0:tok, :] = column
        flat = jnp.transpose(stats[...])[0:8]
        if k == 0:
            got_stats[n] = flat
        else:
            share_stats[n] = flat
            for c in share_copy(head, k):
                c.start()

    def combine(head):
        base = head * X_RING
        for k in range(1, X_RING):
            for c in share_copy(head, k):
                c.wait_recv()
        lse = [got_stats[base + k] for k in range(X_RING)]
        peak = functools.reduce(jnp.maximum, lse)
        weight = [jnp.exp2(v - peak) for v in lse]
        row = lax.broadcasted_iota(jnp.int32, peak.shape, 0)
        factor = jnp.where(row == 1, -subtract[head], 1.0) / functools.reduce(jnp.add, weight)
        wide = jnp.concatenate(
            [w * factor for w in weight]
            + [jnp.zeros((128 - 8 * X_RING, peak.shape[1]), jnp.float32)],
            0,
        )
        turned = jnp.transpose(wide)[0:tok]
        diff = jnp.zeros((tok, 128), jnp.float32)
        for k in range(X_RING):
            o = got[base + k].astype(jnp.float32)
            for m in range(2):
                diff = diff + turned[:, 8 * k + m : 8 * k + m + 1] * o[:, 128 * m : 128 * m + 128]
        spread = jnp.mean(diff * diff, -1, keepdims=True)
        normed = diff * lax.rsqrt(spread + 1e-06) * head_gain[...]
        attended[:, :, 128 * head : 128 * head + 128] = normed.reshape(
            heads, tok // heads, 128
        ).astype(jnp.bfloat16)

    arrived(1, 0)
    start_step(2, 0)
    query_copies[1].wait_recv()
    absorb(0, 1, 0, 256)
    absorb(1, 1, 0, 256)
    query_copies[3].wait_recv()
    query_copies[2].wait_recv()
    absorb(0, 0, 0, 256)
    absorb(1, 0, 0, 256)
    arrived(1, 1)
    start_step(2, 1)
    absorb_both(0, 256, 512)
    absorb_both(1, 256, 512)
    arrived(2, 0)
    start_step(3, 0)
    absorb_both(0, 768, 768)
    arrived(2, 1)
    start_step(3, 1)
    absorb_both(1, 768, 768)
    arrived(3, 0)
    start_step(4, 0)
    absorb_both(0, 1536, 512)
    arrived(3, 1)
    start_step(4, 1)
    absorb_both(1, 1536, 512)
    for head in range(2):
        arrived(4, head)
        absorb(head, 0, 2048, 512)
        finish(head, 2)
        finish(head, 1)
        absorb(head, 1, 2048, 512)
        finish(head, 3)
        finish(head, 0)
    for head in range(2):
        combine(head)

    def head_copy(k):
        return remote(
            attended.at[lax.rem(tp + k, heads)], gathered.at[tp], a_send.at[k], a_recv.at[k],
            along_tp(k),
        )

    for k in range(1, heads):
        head_copy(k).start()
    gathered[pl.ds(tp, 1)] = attended[pl.ds(tp, 1)]
    for k in range(1, heads):
        head_copy(k).wait_recv()
    out[...] = gathered[...]
    for c in ring.values():
        c.wait_send()
    for c in query_copies.values():
        c.wait_send()
    for head in range(2):
        for k in range(1, X_RING):
            for c in share_copy(head, k):
                c.wait_send()
    for k in range(1, heads):
        head_copy(k).wait_send()


def attend(
    query_narrow, key_narrow, value_narrow, query_wide, key_wide, value_wide, subtract_narrow,
    subtract_wide, head_gain,
):
    tok = query_narrow.shape[0]
    heads = lax.axis_size("tp")
    lanes = (tok + 127) // 128 * 128
    vmem = pl.BlockSpec(memory_space=pltpu.VMEM)
    hbm = pl.BlockSpec(memory_space=pl.ANY)
    dma = pltpu.SemaphoreType.DMA
    bf16, f32 = jnp.bfloat16, jnp.float32
    return pl.pallas_call(
        functools.partial(attend_kernel, tok),
        out_shape=jax.ShapeDtypeStruct((heads, tok // heads, 256), bf16),
        in_specs=[hbm] * 6 + [pl.BlockSpec(memory_space=pltpu.SMEM), vmem],
        out_specs=vmem,
        scratch_shapes=[
            pltpu.VMEM((X_RING * tok, 384), bf16),
            pltpu.VMEM((Z_RING * tok, ROW), bf16),
            pltpu.VMEM((4, X_RING * tok, 128), f32),
            pltpu.VMEM((4, X_RING * tok, 256), f32),
            pltpu.VMEM((lanes, 128), f32),
            pltpu.VMEM((2 * X_RING, tok, 256), bf16),
            pltpu.VMEM((2 * X_RING, 8, lanes), f32),
            pltpu.VMEM((2 * X_RING, tok, 256), bf16),
            pltpu.VMEM((2 * X_RING, 8, lanes), f32),
            pltpu.VMEM((heads, tok // heads, 256), bf16),
            pltpu.VMEM((heads, tok // heads, 256), bf16),
            dma((6,)),
            dma((X_RING,)),
            dma((X_RING,)),
            dma((2 * Z_RING,)),
            dma((2 * Z_RING,)),
            dma((2 * X_RING,)),
            dma((2 * X_RING,)),
            dma((2 * X_RING,)),
            dma((2 * X_RING,)),
            dma((heads,)),
            dma((heads,)),
        ],
        compiler_params=pltpu.CompilerParams(
            collective_id=0, has_side_effects=True, vmem_limit_bytes=56 * 1024 * 1024
        ),
        name="attend",
    )(
        query_narrow, key_narrow, value_narrow, query_wide, key_wide, value_wide,
        jnp.concatenate([subtract_narrow, subtract_wide]), head_gain.reshape(1, -1),
    )


def mixed_heads(attended, out_narrow, out_wide):
    rows = attended.shape[1]
    turned = jnp.transpose(attended, (1, 0, 2))
    narrow = turned[:, :, :128].reshape(rows, -1)
    wide = turned[:, :, 128:].reshape(rows, -1)
    return jnp.dot(narrow, out_narrow, preferred_element_type=jnp.float32) + jnp.dot(
        wide, out_wide, preferred_element_type=jnp.float32
    )


def on_device(
    residual,
    query_narrow,
    key_narrow,
    value_narrow,
    query_wide,
    key_wide,
    value_wide,
    subtract_narrow,
    subtract_wide,
    head_gain,
    out_narrow,
    out_wide,
    norm1_gain,
    norm2_gain,
    expert_ids,
    expert_weight,
    gate_proj,
    up_proj,
    down_proj,
):
    attended = attend(
        query_narrow, key_narrow, value_narrow, query_wide, key_wide, value_wide,
        subtract_narrow, subtract_wide, head_gain,
    )
    mix = mixed_heads(attended, out_narrow, out_wide)
    hidden = layer_norm(residual_scale * residual.astype(jnp.float32) + mix, norm1_gain).astype(
        jnp.bfloat16
    )
    local_rows, top_count = expert_ids.shape
    experts = lax.axis_size("sp")
    capacity = max(2, 3 * local_rows * top_count // (2 * experts))
    flat_ids = expert_ids.reshape(-1)
    onehot = (flat_ids[:, None] == jnp.arange(experts, dtype=jnp.int32)[None, :]).astype(jnp.int32)
    before = jnp.cumsum(onehot, 0) - onehot
    position = jnp.sum(before * onehot, 1)
    slots = (flat_ids * capacity + position).reshape(local_rows, top_count)
    dispatch_table = jnp.any(
        jnp.arange(experts * capacity, dtype=jnp.int32)[:, None, None] == slots[None], -1
    ).astype(jnp.bfloat16)
    outgoing = jnp.dot(dispatch_table, hidden, preferred_element_type=jnp.float32).astype(
        jnp.bfloat16
    )
    outgoing = outgoing.reshape(experts, capacity, -1)

    def run_expert(received):
        gathered = lax.all_gather(received, "tp", axis=1, tiled=True)
        flat_rows = gathered.reshape(-1, gathered.shape[2])
        gate_part = jnp.dot(flat_rows, gate_proj[0], preferred_element_type=jnp.float32)
        up_part = jnp.dot(flat_rows, up_proj[0], preferred_element_type=jnp.float32)
        inner = (jax.nn.silu(gate_part) * up_part).astype(jnp.bfloat16)
        partial_out = jnp.dot(inner, down_proj[0], preferred_element_type=jnp.float32).reshape(
            gathered.shape
        )
        summed = lax.psum_scatter(
            partial_out.astype(jnp.bfloat16), "tp", scatter_dimension=1, tiled=True
        )
        return lax.all_to_all(summed, "sp", split_axis=0, concat_axis=0, tiled=True)

    returned = items_in_groups(outgoing, "sp", 0, 0, run_expert, 1, 1)
    returned_flat = returned.reshape(experts * capacity, -1)
    picked = returned_flat[slots].astype(jnp.float32)
    routed = jnp.sum(expert_weight[..., None] * picked, 1)
    return layer_norm(residual_scale * hidden.astype(jnp.float32) + routed, norm2_gain).astype(
        jnp.bfloat16
    )


def solution(mesh):
    placed = (
        P(("sp", "tp"), None),
        P("sp", "tp"),
        P("sp", "tp"),
        P("sp", "tp"),
        P("sp", "tp"),
        P("sp", "tp"),
        P("sp", "tp"),
        P("tp"),
        P("tp"),
        P(),
        P(),
        P(),
        P(),
        P(),
        P(("sp", "tp"), None),
        P(("sp", "tp"), None),
        P("sp", None, "tp"),
        P("sp", None, "tp"),
        P("sp", "tp", None),
    )
    return jax.shard_map(
        on_device, mesh=mesh, in_specs=placed, out_specs=P(("sp", "tp"), None), check_vma=False
    )
```

time: 425 us -> 220 us (0.52)
  waiting for transfers between devices: 192 us -> 78.5 us
  matrix products: 87.6 us -> 7.29 us
  Pallas kernels: 0 us -> 66.7 us
  local copies, waits for them, and re-layouts: 64.1 us -> 13.8 us
  other arithmetic: 22.6 us -> 3.59 us
  starting transfers between devices: 14.8 us -> 10.4 us
    all_gather x2 -> x0, waiting for transfers between devices: 97.2 us -> none  [in_one_piece(): lax.all_gather(both, axis, axis=dim, tiled=True)]
    dot_general x66 -> x2, matrix products: 83.1 us -> 3.97 us  [the longest x1 3.01 us: mixed_heads(): jnp.dot(narrow, out_narrow, preferred_element_type=jnp.float32)]
    pallas_call x0 -> x1, Pallas kernels: none -> 66.7 us  [attend(): pl.pallas_call(functools.partial(attend_kernel, tok), out_shape=jax.Shape...]
    dynamic_slice x64 -> x0, local copies, waits for them, and re-layouts: 36.8 us -> none  [one_block(): lax.dynamic_slice_in_dim(key_piece, step_index * span, span, 0)]
    all_to_all x1 -> x0, waiting for transfers between devices: 17.8 us -> none  [sent_and_summed(): lax.all_to_all(in_blocks(value, dim, devices), axis, 0, 0, tiled=True)]
    reduce_sum x35 -> x0, other arithmetic: 14.8 us -> none  [the longest x32 14.3 us: one_block(): total = total * shrink + jnp.sum(expo, -1)]
    split x3 -> x0, local copies, waits for them, and re-layouts: 11.3 us -> none  [in_one_piece(): jnp.split(lax.all_gather(both, axis, axis=dim, tiled=True), ends, axis=al...]
    all_to_all x1 -> x0, starting transfers between devices: 4.42 us -> none  [sent_and_summed(): lax.all_to_all(in_blocks(value, dim, devices), axis, 0, 0, tiled=True)]
  transfers between devices with their start and end apart: 6 -> 3, of which waited for: 6 -> 3; matrix products, arithmetic and copies ran while one was open for 20% -> 0% of each run, Pallas kernels for 0% -> 0%
where the time goes in v1:
time: 220 us; the launch traced here: 219 us
  waiting for transfers between devices  78.5 us (36%)
  Pallas kernels  66.7 us (30%)
  blocking collectives  23.1 us (10%)
  between operations  15.6 us (7%)
  local copies, waits for them, and re-layouts  13.8 us (6%)
  starting transfers between devices  10.4 us (5%)
  matrix products  7.29 us (3%)
  other arithmetic  3.59 us (2%)
    pallas_call x1, Pallas kernels, attend(): pl.pallas_call(functools.partial(attend_kernel, tok), out_shape=jax.Shape...  66.7 us
    reduce_scatter x1, waiting for transfers between devices, run_expert(): lax.psum_scatter(partial_out.astype(jnp.bfloat16), 'tp', scatter_dimensio...  38.6 us
    all_gather x1, waiting for transfers between devices, run_expert(): gathered = lax.all_gather(received, 'tp', axis=1, tiled=True)  26.2 us
    all_to_all x1, blocking collectives, items_in_groups(): lax.all_to_all(group, axis, split_axis=split_dim, concat_axis=concat_dim,...  23.1 us
    all_to_all x1, waiting for transfers between devices, run_expert(): return lax.all_to_all(summed, 'sp', split_axis=0, concat_axis=0, tiled=True)  13.6 us
    all_to_all x1, starting transfers between devices, run_expert(): return lax.all_to_all(summed, 'sp', split_axis=0, concat_axis=0, tiled=True)  10.1 us
  transfers between devices with their start and end apart: 3, of which 3 were waited for; matrix products, arithmetic and copies ran while one was open for 0% of the time, Pallas kernels for 0%

profile of v1, /device:TPU:2, one launch (start us, length us, event | category | flops | bytes accessed | tf_op | source)
XLA Modules:
  0.0 219.1 jit_solution(13506455852774317177)
XLA Ops:
  8.5 0.6 pad_maximum_fusion.subtract
  9.1 66.7 %attend.1 = bf16[8,40,256]{2,1,0:T(8,128)(2,1)} custom-call(bf16[320,128]{1,0:T(8,128)(2,1)} %query_narrow.1, bf16[320,128]{1,0:T(8,128)(2,1)} %key_narrow.1, bf16[320,128]{1,0:T(8,128)(2,1)} %value_narrow.1, bf16[320,256]{1,0:T(8,128)(2,1)} %query_wide.1, bf16[320,256]{1,0:T(8,128)(2,1)} %key_wide.1, bf16[320,128]{1,0:T(8,128)(2,1)} %value_wide.1, ...), custom_call_target="tpu_custom_call" | custom-call | tf_op jit(solution)/shard_map/attend/pallas_call | solution.py:362
  75.9 0.9 slice_bitcast_fusion
  76.8 3.0 %fusion.9 = f32[40,2048]{1,0:T(8,128)S(1)} fusion(bf16[1024,2048]{1,0:T(8,128)(2,1)} %param.29, bf16[8,5,8,128]{3,2,1,0:T(8,128)(2,1)S(1)} %get-tuple-element.8), kind=kOutput, calls=%fused_computation.20 | convolution fusion | flops 167772160 | bytes 4603904 | tf_op jit(solution)/shard_map/dot_general | solution.py:406
  79.8 0.0 copy-start.5
  79.8 0.0 copy-start.3
  79.9 1.0 fusion.14
  80.8 0.2 multiply_reduce_fusion.2
  81.1 0.1 copy.73
  81.2 0.1 eq.29
  81.3 0.1 fusion.12
  81.4 0.1 reduce_window_sum.11
  81.5 0.2 select_reduce_fusion
  81.7 0.1 reduce_sum.59
  81.8 0.1 copy.74
  81.9 0.1 fusion.13
  82.0 0.3 convolution_convert_fusion.1
  82.3 0.2 reshape.60
  82.6 23.1 %all_to_all.10 = bf16[32,3,2048]{2,1,0:T(4,128)(2,1)S(1)} all-to-all(bf16[32,3,2048]{2,1,0:T(4,128)(2,1)S(1)} %reshape.60), channel_id=1, replica_groups=mesh['sp'=32,'tp'=8] {'sp'}, dimensions={0} | all-to-all | bytes 786432 | tf_op jit(solution)/shard_map/all_to_all | solution.py:27
  105.7 1.0 copy.75
  106.7 0.0 all-gather.2.cloned.1.call-update
  106.8 0.0 copy-start.7
  106.8 0.3 reduce-scatter.2.cloned.1.call-start
  107.1 26.2 %all-gather.2.cloned.1.call-done = bf16[32,24,2048]{2,0,1:T(8,128)(2,1)} async-done(((bf16[32,3,2048]{2,0,1:T(8,128)(2,1)}), bf16[32,24,2048]{2,0,1:T(8,128)(2,1)}) %all-gather.2.cloned.1.call-update) | async-done | bytes 3145744 | tf_op jit(solution)/shard_map/all_gather | solution.py:457
  133.3 3.6 %copy.76 = bf16[32,24,2048]{2,1,0:T(8,128)(2,1)S(1)} copy(bf16[32,24,2048]{2,0,1:T(8,128)(2,1)} %all-gather.2.cloned.1.call-done) | data formatting | bytes 6291456 | tf_op jit(solution)/shard_map/all_gather | solution.py:457
  136.9 0.0 copy-start.8
  136.9 0.0 copy-done.7
  136.9 1.0 fusion.4
  137.9 0.2 copy-done.8
  138.1 1.0 fusion.1
  139.1 1.0 convolution_convert_fusion
  140.1 3.4 %copy.77 = bf16[32,24,2048]{2,0,1:T(8,128)(2,1)} copy(bf16[32,24,2048]{2,1,0:T(8,128)(2,1)S(1)} %convolution_convert_fusion) | data formatting | bytes 6291456 | tf_op jit(solution)/shard_map/convert_element_type | solution.py:466
  143.5 0.0 reduce-scatter.2.cloned.1.call-update
  143.6 38.6 %reduce-scatter.2.cloned.1.call-done = bf16[32,3,2048]{2,0,1:T(8,128)(2,1)} async-done(((bf16[32,24,2048]{2,0,1:T(8,128)(2,1)}), bf16[32,3,2048]{2,0,1:T(8,128)(2,1)}) %reduce-scatter.2.cloned.1.call-update) | async-done | bytes 393232 | tf_op jit(solution)/shard_map/reduce_scatter | solution.py:465
  182.1 2.1 copy.78
  184.3 10.1 %all-to-all-start.1 = ((bf16[32,3,2048]{2,1,0:T(4,128)(2,1)}), bf16[32,3,2048]{2,1,0:T(4,128)(2,1)S(1)}, u32[]{:S(2)}, u32[]{:S(2)}) async-start(bf16[32,3,2048]{2,1,0:T(4,128)(2,1)} %copy.78), calls=%async_computation.2 | async-start | bytes 1048576 | tf_op jit(solution)/shard_map/all_to_all | solution.py:468
  194.4 0.1 copy.79
  194.5 0.1 reshape.65
  194.6 0.1 copy.72
  194.7 13.6 %all-to-all-done.1 = bf16[32,3,2048]{2,1,0:T(4,128)(2,1)S(1)} async-done(((bf16[32,3,2048]{2,1,0:T(4,128)(2,1)}), bf16[32,3,2048]{2,1,0:T(4,128)(2,1)S(1)}, u32[]{:S(2)}, u32[]{:S(2)}) %all-to-all-start.1) | async-done | bytes 393248 | tf_op jit(solution)/shard_map/all_to_all | solution.py:468
  208.4 0.3 reshape.62
  208.7 0.0 copy-start.4
  208.7 0.8 gather_fusion
  209.5 0.4 reshape.73
  209.9 0.9 multiply_reduce_fusion
  210.9 0.2 fusion.6
  211.1 0.3 multiply_reduce_fusion.1
  211.4 0.8 multiply_convert_fusion
  (18 shorter events, 0.1 us)
Async XLA Ops:
  6.5 132.6 %copy-start = (bf16[1,256,2048]{2,1,0:T(8,128)(2,1)S(1)}, bf16[1,256,2048]{2,1,0:T(8,128)(2,1)}, u32[]{:S(2)}) copy-start(bf16[1,256,2048]{2,1,0:T(8,128)(2,1)} %param.37) | copy-start | bytes 3145732
  6.5 73.3 %copy-start.2 = (bf16[40,2048]{1,0:T(8,128)(2,1)S(1)}, bf16[40,2048]{1,0:T(8,128)(2,1)}, u32[]{:S(2)}) copy-start(bf16[40,2048]{1,0:T(8,128)(2,1)} %param.19) | copy-start | bytes 491524
  6.5 126.7 %all-gather.2.cloned.1.call-start = ((), (), s32[]{:S(2)}) async-start(), calls=%async_computation.3 | async-start | bytes 3538944 | tf_op jit(solution)/shard_map/all_gather | solution.py:457
  6.5 73.3 %copy-start.1 = (bf16[1024,2048]{1,0:T(8,128)(2,1)S(1)}, bf16[1024,2048]{1,0:T(8,128)(2,1)}, u32[]{:S(2)}) copy-start(bf16[1024,2048]{1,0:T(8,128)(2,1)} %param.30) | copy-start | bytes 12582916
  79.8 1.2 copy-start.5
  79.8 2.1 copy-start.3
  106.8 30.1 %copy-start.7 = (bf16[1,2048,256]{2,1,0:T(8,128)(2,1)S(1)}, bf16[1,2048,256]{2,1,0:T(8,128)(2,1)}, u32[]{:S(2)}) copy-start(bf16[1,2048,256]{2,1,0:T(8,128)(2,1)} %param.35) | copy-start | bytes 3145732
  106.8 75.4 %reduce-scatter.2.cloned.1.call-start = ((), (), s32[]{:S(2)}) async-start(), calls=%async_computation.4 | async-start | bytes 3538944 | tf_op jit(solution)/shard_map/reduce_scatter | solution.py:465
  136.9 1.2 copy-start.8
  143.5 51.1 %copy-start.6 = (f32[40,2]{0,1:T(2,128)S(1)}, f32[40,2]{0,1:T(2,128)}, u32[]{:S(2)}) copy-start(f32[40,2]{0,1:T(2,128)} %param.34) | copy-start | bytes 964
  184.3 24.1 %all-to-all-start.1 = ((bf16[32,3,2048]{2,1,0:T(4,128)(2,1)}), bf16[32,3,2048]{2,1,0:T(4,128)(2,1)S(1)}, u32[]{:S(2)}, u32[]{:S(2)}) async-start(bf16[32,3,2048]{2,1,0:T(4,128)(2,1)} %copy.78), calls=%async_computation.2 | async-start | bytes 1048576 | tf_op jit(solution)/shard_map/all_to_all | solution.py:468
  208.7 2.7 %copy-start.4 = (f32[2048]{0:T(1024)S(1)}, f32[2048]{0:T(1024)}, u32[]{:S(2)}) copy-start(f32[2048]{0:T(1024)} %param.32) | copy-start | bytes 24580
Sparse Core Ops, SparseCore 0:
  106.9 26.3 all-gather.1
  143.7 38.4 reduce-scatter.1

commit v2 on v1

--- a/solution.py
+++ b/solution.py
@@ -9,27 +9,6 @@
 
 residual_scale = 2.0**0.5
 MESH = pl.DeviceIdType.MESH
-
-
-def items_in_groups(value, axis, split_dim, concat_dim, work, item_dim, out_dim):
-    items = jax.tree.leaves(value)[0].shape[item_dim]
-    count = 2 if items % 2 == 0 else 1
-    outs = []
-    for k in range(count):
-        group = jax.tree.map(
-            lambda a: lax.slice_in_dim(
-                a, k * (items // count), (k + 1) * (items // count), axis=item_dim
-            ),
-            value,
-        )
-        outs.append(
-            work(
-                lax.all_to_all(
-                    group, axis, split_axis=split_dim, concat_axis=concat_dim, tiled=True
-                )
-            )
-        )
-    return jax.tree.map(lambda *parts: jnp.concatenate(parts, axis=out_dim), *outs)
 
 
 def layer_norm(values, gain):
@@ -408,6 +387,368 @@
     )
 
 
+Y_RING = 4
+STEPS_Z = (0, 1, 7, 4, 2, 6, 3, 5)
+GROUPS = 2
+LANES = 128
+
+
+def to_tiles(values, words, target, first):
+    rows, width = values.shape
+    tall = width // LANES
+    for j in range(tall):
+        words[pl.ds(j, rows, stride=tall), :] = values[:, LANES * j : LANES * (j + 1)]
+    flat = words[0 : rows * tall, :]
+    target[first : first + rows] = flat.reshape(rows, tall, LANES).astype(jnp.bfloat16)
+
+
+def from_tiles(source, first, rows, words, target):
+    tall = source.shape[1]
+    flat = source[first : first + rows].astype(jnp.float32)
+    words[0 : rows * tall, :] = flat.reshape(rows * tall, LANES)
+    for j in range(tall):
+        target[:, LANES * j : LANES * (j + 1)] = words[pl.ds(j, rows, stride=tall), :].astype(
+            jnp.bfloat16
+        )
+
+
+def experts_kernel(
+    capacity,
+    hidden,
+    slots_across,
+    slots_down,
+    expert_weight,
+    norm2_gain,
+    gate_proj,
+    up_proj,
+    down_proj,
+    out,
+    gate,
+    up,
+    down,
+    words,
+    outgoing,
+    received,
+    gathered,
+    partial,
+    from_core,
+    half_sum,
+    from_half,
+    whole_sum,
+    from_side,
+    results,
+    returned,
+    returned_rows,
+    w_sem,
+    d_send,
+    d_recv,
+    g_send,
+    g_recv,
+    c_send,
+    c_recv,
+    h_send,
+    h_recv,
+    f_send,
+    f_recv,
+    r_send,
+    r_recv,
+):
+    sp = lax.axis_index("sp")
+    tp = lax.axis_index("tp")
+    z, x = sp // X_RING, sp % X_RING
+    y, core = tp // 2, tp % 2
+    experts = Z_RING * X_RING
+    width = hidden.shape[1]
+    half = width // 2
+    f32, bf16 = jnp.float32, jnp.bfloat16
+
+    def expert_at(dz, dx):
+        return lax.rem(z + dz, Z_RING) * X_RING + lax.rem(x + dx, X_RING)
+
+    def along_y(k):
+        return (sp, lax.rem(y + k, Y_RING) * 2 + core)
+
+    sibling = (sp, y * 2 + 1 - core)
+    loads = [
+        pltpu.make_async_copy(src.at[0], dst, w_sem.at[i])
+        for i, (src, dst) in enumerate(((gate_proj, gate), (up_proj, up), (down_proj, down)))
+    ]
+    for c in loads:
+        c.start()
+    others = [(dz, dx) for dz in STEPS_Z for dx in range(X_RING) if dz or dx]
+    peers = [(expert_at(dz, dx), tp) for dz, dx in others]
+    peers = peers + [sibling, along_y(1), along_y(Y_RING - 1)]
+    barrier = pltpu.get_barrier_semaphore()
+    for peer in peers:
+        pl.semaphore_signal(barrier, inc=1, device_id=peer, device_id_type=MESH)
+
+    local_rows, top_count = expert_weight.shape
+    row = lax.broadcasted_iota(jnp.int32, (experts * capacity, local_rows), 0)
+    table = jnp.zeros(row.shape, f32)
+    for c in range(top_count):
+        table = jnp.where(row == slots_across[c : c + 1, :], 1.0, table)
+    rows = jnp.dot(table.astype(bf16), hidden[...], preferred_element_type=f32)
+    to_tiles(rows, words, outgoing, 0)
+    pl.semaphore_wait(barrier, len(peers))
+
+    def remote(src, dst, send, recv, peer):
+        return pltpu.make_async_remote_copy(
+            src_ref=src, dst_ref=dst, send_sem=send, recv_sem=recv, device_id=peer,
+            device_id_type=MESH,
+        )
+
+    def place(dz, dx):
+        return STEPS_Z.index(dz % Z_RING) * X_RING + dx % X_RING
+
+    def dispatch_copy(dz, dx):
+        e = expert_at(dz, dx)
+        p = place(-dz, -dx)
+        return remote(
+            outgoing.at[pl.ds(e * capacity, capacity)],
+            received.at[pl.ds(p * capacity, capacity)],
+            d_send.at[p], d_recv.at[p], (e, tp),
+        )
+
+    def return_copy(dz, dx):
+        p = place(dz, dx)
+        return remote(
+            results.at[pl.ds(p * capacity, capacity)],
+            returned.at[pl.ds(sp * capacity, capacity)],
+            r_send.at[p], r_recv.at[p], (expert_at(dz, dx), tp),
+        )
+
+    per_group = len(STEPS_Z) // GROUPS
+    steps_of = [STEPS_Z[g * per_group : (g + 1) * per_group] for g in range(GROUPS)]
+    hops = [[(dz, dx) for dz in steps_of[g] for dx in range(X_RING)] for g in range(GROUPS)]
+    block = per_group * X_RING * capacity
+    low, high = pl.ds(0, half), pl.ds(half, half)
+
+    for g in range(GROUPS):
+        for dz, dx in hops[g]:
+            if dz or dx:
+                dispatch_copy(dz, dx).start()
+
+    def gather_copies(g):
+        at = lambda s, c=None: gathered.at[g, s] if c is None else gathered.at[g, s, :, c]
+        right, left = along_y(1), along_y(Y_RING - 1)
+        plan = {
+            "core0": (at(0), at(1), sibling),
+            "right": (at(0), at(6), right),
+            "left": (at(0), at(2), left),
+            "right2": (at(6, low), at(4, low), right),
+            "left2": (at(2, high), at(4, high), left),
+            "core1": (at(2), at(3), sibling),
+            "core3": (at(6), at(7), sibling),
+            "core2": (at(4), at(5), sibling),
+        }
+        return {
+            name: remote(src, dst, g_send.at[g, i], g_recv.at[g, i], peer)
+            for i, (name, (src, dst, peer)) in enumerate(plan.items())
+        }
+
+    gathers = [gather_copies(g) for g in range(GROUPS)]
+
+    def core_copy(g, k):
+        return remote(
+            partial.at[g, 2 * k + 1], from_core.at[g, k], c_send.at[g, k], c_recv.at[g, k], sibling
+        )
+
+    def half_copy(g, way):
+        return remote(
+            half_sum.at[g, way], from_half.at[g, way], h_send.at[g, way], h_recv.at[g, way],
+            along_y(Y_RING - 1 if way else 1),
+        )
+
+    def side_copy(g, way, part):
+        cols = high if part else low
+        return remote(
+            whole_sum.at[g, way, :, cols], from_side.at[g, way, :, cols],
+            f_send.at[g, way, part], f_recv.at[g, way, part], along_y(Y_RING - 1 if way else 1),
+        )
+
+    def open_group(g):
+        for dz, dx in hops[g]:
+            p = place(dz, dx)
+            if dz or dx:
+                dispatch_copy(-dz % Z_RING, -dx % X_RING).wait_recv()
+            else:
+                received[p * capacity : (p + 1) * capacity] = outgoing[
+                    pl.ds(sp * capacity, capacity)
+                ]
+        from_tiles(received, g * block, block, words, gathered.at[g, 0])
+        for name in ("right", "left", "core0"):
+            gathers[g][name].start()
+
+    def pass_on(g):
+        gathers[g]["right"].wait_recv()
+        gathers[g]["right2"].start()
+        gathers[g]["left"].wait_recv()
+        gathers[g]["left2"].start()
+        gathers[g]["core3"].start()
+        gathers[g]["core1"].start()
+
+    def close_gather(g):
+        gathers[g]["right2"].wait_recv()
+        gathers[g]["left2"].wait_recv()
+        gathers[g]["core2"].start()
+        for name in ("core0", "core1", "core3", "core2"):
+            gathers[g][name].wait_recv()
+
+    def multiply(g):
+        flat = gathered[g].reshape(-1, width)
+        gate_part = jnp.dot(flat, gate[...], preferred_element_type=f32)
+        up_part = jnp.dot(flat, up[...], preferred_element_type=f32)
+        inner = (gate_part * jax.nn.sigmoid(gate_part) * up_part).astype(bf16)
+        share = jnp.dot(inner, down[...], preferred_element_type=f32).astype(bf16)
+        partial[g] = share.reshape(2 * Y_RING, block, width)
+        for k in (2, 1, 3, 0):
+            core_copy(g, k).start()
+
+    def both_cores(g, k, cols):
+        return partial[g, 2 * k, :, cols].astype(f32) + from_core[g, k, :, cols].astype(f32)
+
+    def send_halves(g):
+        core_copy(g, 2).wait_recv()
+        half_sum[g, 0] = both_cores(g, 2, low).astype(bf16)
+        half_sum[g, 1] = both_cores(g, 2, high).astype(bf16)
+        half_copy(g, 0).start()
+        half_copy(g, 1).start()
+        core_copy(g, 1).wait_recv()
+        whole_sum[g, 0, :, high] = both_cores(g, 1, high).astype(bf16)
+        side_copy(g, 0, 1).start()
+        core_copy(g, 3).wait_recv()
+        whole_sum[g, 1, :, low] = both_cores(g, 3, low).astype(bf16)
+        side_copy(g, 1, 0).start()
+
+    def send_sides(g):
+        half_copy(g, 0).wait_recv()
+        whole_sum[g, 0, :, low] = (both_cores(g, 1, low) + from_half[g, 0].astype(f32)).astype(bf16)
+        side_copy(g, 0, 0).start()
+        half_copy(g, 1).wait_recv()
+        whole_sum[g, 1, :, high] = (both_cores(g, 3, high) + from_half[g, 1].astype(f32)).astype(
+            bf16
+        )
+        side_copy(g, 1, 1).start()
+
+    def give_back(g):
+        core_copy(g, 0).wait_recv()
+        for way in range(2):
+            for part in range(2):
+                side_copy(g, way, part).wait_recv()
+        total = (
+            both_cores(g, 0, slice(None))
+            + from_side[g, 0].astype(f32)
+            + from_side[g, 1].astype(f32)
+        )
+        to_tiles(total, words, results, g * block)
+        for dz, dx in hops[g]:
+            p = place(dz, dx)
+            if dz or dx:
+                return_copy(dz, dx).start()
+            else:
+                returned[pl.ds(sp * capacity, capacity)] = results[
+                    p * capacity : (p + 1) * capacity
+                ]
+
+    open_group(0)
+    pass_on(0)
+    open_group(1)
+    close_gather(0)
+    for c in loads:
+        c.wait()
+    multiply(0)
+    pass_on(1)
+    send_halves(0)
+    close_gather(1)
+    multiply(1)
+    send_sides(0)
+    send_halves(1)
+    give_back(0)
+    send_sides(1)
+    give_back(1)
+    for dz, dx in others:
+        return_copy(-dz % Z_RING, -dx % X_RING).wait_recv()
+    from_tiles(returned, 0, experts * capacity, words, returned_rows)
+    column = lax.broadcasted_iota(jnp.int32, (local_rows, experts * capacity), 1)
+    routed = jnp.zeros((local_rows, width), f32)
+    for c in range(top_count):
+        pick = (column == slots_down[:, c : c + 1]).astype(f32).astype(bf16)
+        picked = jnp.dot(pick, returned_rows[...], preferred_element_type=f32)
+        routed = routed + expert_weight[:, c : c + 1] * picked
+    out[...] = layer_norm(
+        residual_scale * hidden[...].astype(f32) + routed, norm2_gain[...]
+    ).astype(bf16)
+    for dz, dx in others:
+        dispatch_copy(dz, dx).wait_send()
+        return_copy(dz, dx).wait_send()
+    for g in range(GROUPS):
+        for c in gathers[g].values():
+            c.wait_send()
+        for k in range(Y_RING):
+            core_copy(g, k).wait_send()
+        for way in range(2):
+            half_copy(g, way).wait_send()
+            for part in range(2):
+                side_copy(g, way, part).wait_send()
+
+
+def run_experts(hidden, slots, capacity, expert_weight, norm2_gain, gate_proj, up_proj, down_proj):
+    local_rows, width = hidden.shape
+    experts = Z_RING * X_RING
+    inner = gate_proj.shape[2]
+    count = experts * capacity
+    block = count // GROUPS
+    tall = width // LANES
+    vmem = pl.BlockSpec(memory_space=pltpu.VMEM)
+    hbm = pl.BlockSpec(memory_space=pl.ANY)
+    dma = pltpu.SemaphoreType.DMA
+    bf16, f32 = jnp.bfloat16, jnp.float32
+    return pl.pallas_call(
+        functools.partial(experts_kernel, capacity),
+        out_shape=jax.ShapeDtypeStruct((local_rows, width), bf16),
+        in_specs=[vmem] * 5 + [hbm] * 3,
+        out_specs=vmem,
+        scratch_shapes=[
+            pltpu.VMEM((width, inner), bf16),
+            pltpu.VMEM((width, inner), bf16),
+            pltpu.VMEM((inner, width), bf16),
+            pltpu.VMEM((count * tall, LANES), f32),
+            pltpu.VMEM((count, tall, LANES), bf16),
+            pltpu.VMEM((count, tall, LANES), bf16),
+            pltpu.VMEM((GROUPS, 2 * Y_RING, block, width), bf16),
+            pltpu.VMEM((GROUPS, 2 * Y_RING, block, width), bf16),
+            pltpu.VMEM((GROUPS, Y_RING, block, width), bf16),
+            pltpu.VMEM((GROUPS, 2, block, width // 2), bf16),
+            pltpu.VMEM((GROUPS, 2, block, width // 2), bf16),
+            pltpu.VMEM((GROUPS, 2, block, width), bf16),
+            pltpu.VMEM((GROUPS, 2, block, width), bf16),
+            pltpu.VMEM((count, tall, LANES), bf16),
+            pltpu.VMEM((count, tall, LANES), bf16),
+            pltpu.VMEM((count, width), bf16),
+            dma((3,)),
+            dma((experts,)),
+            dma((experts,)),
+            dma((GROUPS, 8)),
+            dma((GROUPS, 8)),
+            dma((GROUPS, Y_RING)),
+            dma((GROUPS, Y_RING)),
+            dma((GROUPS, 2)),
+            dma((GROUPS, 2)),
+            dma((GROUPS, 2, 2)),
+            dma((GROUPS, 2, 2)),
+            dma((experts,)),
+            dma((experts,)),
+        ],
+        compiler_params=pltpu.CompilerParams(
+            collective_id=1, has_side_effects=True, vmem_limit_bytes=56 * 1024 * 1024
+        ),
+        name="experts",
+    )(
+        hidden, jnp.transpose(slots), slots, expert_weight, norm2_gain.reshape(1, -1), gate_proj,
+        up_proj, down_proj,
+    )
+
+
 def on_device(
     residual,
     query_narrow,
@@ -445,34 +786,8 @@
     before = jnp.cumsum(onehot, 0) - onehot
     position = jnp.sum(before * onehot, 1)
     slots = (flat_ids * capacity + position).reshape(local_rows, top_count)
-    dispatch_table = jnp.any(
-        jnp.arange(experts * capacity, dtype=jnp.int32)[:, None, None] == slots[None], -1
-    ).astype(jnp.bfloat16)
-    outgoing = jnp.dot(dispatch_table, hidden, preferred_element_type=jnp.float32).astype(
-        jnp.bfloat16
-    )
-    outgoing = outgoing.reshape(experts, capacity, -1)
-
-    def run_expert(received):
-        gathered = lax.all_gather(received, "tp", axis=1, tiled=True)
-        flat_rows = gathered.reshape(-1, gathered.shape[2])
-        gate_part = jnp.dot(flat_rows, gate_proj[0], preferred_element_type=jnp.float32)
-        up_part = jnp.dot(flat_rows, up_proj[0], preferred_element_type=jnp.float32)
-        inner = (jax.nn.silu(gate_part) * up_part).astype(jnp.bfloat16)
-        partial_out = jnp.dot(inner, down_proj[0], preferred_element_type=jnp.float32).reshape(
-            gathered.shape
-        )
-        summed = lax.psum_scatter(
-            partial_out.astype(jnp.bfloat16), "tp", scatter_dimension=1, tiled=True
-        )
-        return lax.all_to_all(summed, "sp", split_axis=0, concat_axis=0, tiled=True)
-
-    returned = items_in_groups(outgoing, "sp", 0, 0, run_expert, 1, 1)
-    returned_flat = returned.reshape(experts * capacity, -1)
-    picked = returned_flat[slots].astype(jnp.float32)
-    routed = jnp.sum(expert_weight[..., None] * picked, 1)
-    return layer_norm(residual_scale * hidden.astype(jnp.float32) + routed, norm2_gain).astype(
-        jnp.bfloat16
+    return run_experts(
+        hidden, slots, capacity, expert_weight, norm2_gain, gate_proj, up_proj, down_proj
     )
 
 

time: 220 us -> 139 us (0.63)
  waiting for transfers between devices: 78.5 us -> 0 us
  Pallas kernels: 66.7 us -> 125 us
  blocking collectives: 23.1 us -> 0 us
  between operations: 15.6 us -> 1.99 us
  starting transfers between devices: 10.4 us -> 0 us
  local copies, waits for them, and re-layouts: 13.8 us -> 4.28 us
  matrix products: 7.29 us -> 3.98 us
    pallas_call x0 -> x1, Pallas kernels: none -> 58.5 us  [run_experts(): pl.pallas_call(functools.partial(experts_kernel, capacity), out_shape=jax...]
    reduce_scatter x1 -> x0, waiting for transfers between devices: 38.6 us -> none  [run_expert(): lax.psum_scatter(partial_out.astype(jnp.bfloat16), 'tp', scatter_dimensio...]
    all_gather x1 -> x0, waiting for transfers between devices: 26.2 us -> none  [run_expert(): gathered = lax.all_gather(received, 'tp', axis=1, tiled=True)]
    all_to_all x1 -> x0, blocking collectives: 23.1 us -> none  [items_in_groups(): lax.all_to_all(group, axis, split_axis=split_dim, concat_axis=concat_dim,...]
    all_to_all x1 -> x0, waiting for transfers between devices: 13.6 us -> none  [run_expert(): return lax.all_to_all(summed, 'sp', split_axis=0, concat_axis=0, tiled=True)]
    all_to_all x1 -> x0, starting transfers between devices: 10.1 us -> none  [run_expert(): return lax.all_to_all(summed, 'sp', split_axis=0, concat_axis=0, tiled=True)]
    convert_element_type x2 -> x0, local copies, waits for them, and re-layouts: 3.81 us -> none  [the longest x1 3.39 us: run_expert(): partial_out.astype(jnp.bfloat16)]
    all_gather x1 -> x0, local copies, waits for them, and re-layouts: 3.61 us -> none  [run_expert(): gathered = lax.all_gather(received, 'tp', axis=1, tiled=True)]
  transfers between devices with their start and end apart: 3 -> 0, of which waited for: 3 -> 0; matrix products, arithmetic and copies ran while one was open for 0% -> 0% of each run, Pallas kernels for 0% -> 0%
where the time goes in v2:
time: 139 us; the launch traced here: 137 us
  Pallas kernels  125 us (90%)
  local copies, waits for them, and re-layouts  4.28 us (3%)
  matrix products  3.98 us (3%)
  between operations  1.99 us (1%)
  other arithmetic  1.97 us (1%)
    pallas_call x1, Pallas kernels, attend(): pl.pallas_call(functools.partial(attend_kernel, tok), out_shape=jax.Shape...  66.7 us
    pallas_call x1, Pallas kernels, run_experts(): pl.pallas_call(functools.partial(experts_kernel, capacity), out_shape=jax...  58.5 us
    unnamed x16, local copies, waits for them, and re-layouts  3.35 us
    dot_general x1, matrix products, mixed_heads(): jnp.dot(narrow, out_narrow, preferred_element_type=jnp.float32)  3.02 us

profile of v2, /device:TPU:2, one launch (start us, length us, event | category | flops | bytes accessed | tf_op | source)
XLA Modules:
  0.0 137.5 jit_solution(15352762717719665047)
XLA Ops:
  0.0 0.0 copy-start.2
  0.0 0.0 copy-start
  1.9 0.6 pad_maximum_fusion.subtract
  2.5 66.7 %attend.1 = bf16[8,40,256]{2,1,0:T(8,128)(2,1)} custom-call(bf16[320,128]{1,0:T(8,128)(2,1)} %query_narrow.1, bf16[320,128]{1,0:T(8,128)(2,1)} %key_narrow.1, bf16[320,128]{1,0:T(8,128)(2,1)} %value_narrow.1, bf16[320,256]{1,0:T(8,128)(2,1)} %query_wide.1, bf16[320,256]{1,0:T(8,128)(2,1)} %key_wide.1, bf16[320,128]{1,0:T(8,128)(2,1)} %value_wide.1, ...), custom_call_target="tpu_custom_call" | custom-call | tf_op jit(solution)/shard_map/attend/pallas_call | solution.py:341
  69.2 0.9 slice_bitcast_fusion
  70.2 0.0 copy-start.3
  70.2 0.0 copy-start.4
  70.2 3.0 %fusion.3 = f32[40,2048]{1,0:T(8,128)S(1)} fusion(bf16[1024,2048]{1,0:T(8,128)(2,1)} %param.29, bf16[8,5,8,128]{3,2,1,0:T(8,128)(2,1)S(1)} %get-tuple-element.6), kind=kOutput, calls=%fused_computation.6 | convolution fusion | flops 167772160 | bytes 4603904 | tf_op jit(solution)/shard_map/dot_general | solution.py:385
  73.2 0.0 copy-start.5
  73.2 0.0 copy-done.2
  73.2 0.0 copy-done
  73.3 1.0 fusion.7
  74.2 0.2 multiply_reduce_fusion
  74.5 0.0 copy-done.3
  74.5 0.8 multiply_convert_fusion.hidden
  75.2 0.0 copy-done.4
  75.2 0.1 copy.34
  75.3 0.1 eq.15
  75.4 0.1 fusion.6
  75.5 0.1 reduce_window_sum.11
  75.7 0.2 select_reduce_fusion
  75.8 0.1 reduce_sum.32
  76.0 0.1 copy.35
  76.1 0.0 copy-start.1
  76.1 0.6 copy.36.slots_across
  76.7 0.0 copy-done.5
  76.7 0.7 copy.37.expert_weight
  77.4 0.0 copy-done.1
  77.4 58.5 %experts.1 = bf16[40,2048]{1,0:T(8,128)(2,1)} custom-call(bf16[40,2048]{1,0:T(8,128)(2,1)} %multiply_convert_fusion.hidden, s32[2,40]{1,0:T(2,128)} %copy.36.slots_across, s32[40,2]{1,0:T(8,128)} %copy-done.1, f32[40,2]{1,0:T(8,128)} %copy.37.expert_weight, f32[1,2048]{1,0:T(1,128)} %bitcast.20, bf16[1,2048,256]{2,1,0:T(8,128)(2,1)} %gate_proj.1, ...), custom_call_target="tpu_custom_call" | custom-call | tf_op jit(solution)/shard_map/experts/pallas_call | solution.py:706
  135.9 1.6 %copy.53 = bf16[40,2048]{1,0:T(8,128)(2,1)} copy(bf16[40,2048]{1,0:T(8,128)(2,1)} %experts.1) | data formatting | bytes 327680
  (4 shorter events, 0.0 us)
Async XLA Ops:
  0.0 73.2 %copy-start.2 = (bf16[40,2048]{1,0:T(8,128)(2,1)S(1)}, bf16[40,2048]{1,0:T(8,128)(2,1)}, u32[]{:S(2)}) copy-start(bf16[40,2048]{1,0:T(8,128)(2,1)} %param.19) | copy-start | bytes 491524
  0.0 73.2 %copy-start = (bf16[1024,2048]{1,0:T(8,128)(2,1)S(1)}, bf16[1024,2048]{1,0:T(8,128)(2,1)}, u32[]{:S(2)}) copy-start(bf16[1024,2048]{1,0:T(8,128)(2,1)} %param.30) | copy-start | bytes 12582916
  70.2 4.3 %copy-start.3 = (f32[2048]{0:T(1024)S(1)}, f32[2048]{0:T(1024)}, u32[]{:S(2)}) copy-start(f32[2048]{0:T(1024)} %param.31) | copy-start | bytes 24580
  70.2 5.1 %copy-start.4 = (s32[40,2]{0,1:T(2,128)S(1)}, s32[40,2]{0,1:T(2,128)}, u32[]{:S(2)}) copy-start(s32[40,2]{0,1:T(2,128)} %param.33) | copy-start | bytes 964
  73.2 3.5 %copy-start.5 = (f32[40,2]{0,1:T(2,128)S(1)}, f32[40,2]{0,1:T(2,128)}, u32[]{:S(2)}) copy-start(f32[40,2]{0,1:T(2,128)} %param.34) | copy-start | bytes 964
  76.1 1.3 copy-start.1

commit v3 on v2

--- a/solution.py
+++ b/solution.py
@@ -27,16 +27,53 @@
 QPLACE = (3, 1, 0, 2)
 
 
-def attend_kernel(
+Y_RING = 4
+STEPS_Z = (0, 1, 7, 4, 2, 6, 3, 5)
+GROUPS = 2
+LANES = 128
+
+
+def to_tiles(values, words, target, first):
+    rows, width = values.shape
+    tall = width // LANES
+    for j in range(tall):
+        words[pl.ds(j, rows, stride=tall), :] = values[:, LANES * j : LANES * (j + 1)]
+    flat = words[0 : rows * tall, :]
+    target[first : first + rows] = flat.reshape(rows, tall, LANES).astype(jnp.bfloat16)
+
+
+def from_tiles(source, first, rows, words, target):
+    tall = source.shape[1]
+    flat = source[first : first + rows].astype(jnp.float32)
+    words[0 : rows * tall, :] = flat.reshape(rows * tall, LANES)
+    for j in range(tall):
+        target[:, LANES * j : LANES * (j + 1)] = words[pl.ds(j, rows, stride=tall), :].astype(
+            jnp.bfloat16
+        )
+
+
+def layer_kernel(
     tok,
+    capacity,
+    residual,
     query_narrow,
     key_narrow,
     value_narrow,
     query_wide,
     key_wide,
     value_wide,
-    subtract,
+    subtract_narrow,
+    subtract_wide,
     head_gain,
+    out_narrow,
+    out_wide,
+    norm1_gain,
+    norm2_gain,
+    expert_ids,
+    expert_weight,
+    gate_proj,
+    up_proj,
+    down_proj,
     out,
     queries,
     keys,
@@ -48,7 +85,27 @@
     got,
     got_stats,
     attended,
+    gathered_heads,
+    mix_narrow,
+    mix_wide,
+    hidden,
+    picks,
+    gate,
+    up,
+    down,
+    words,
+    outgoing,
+    received,
     gathered,
+    partial,
+    from_core,
+    half_sum,
+    from_half,
+    whole_sum,
+    from_side,
+    results,
+    returned,
+    returned_rows,
     local_sem,
     q_send,
     q_recv,
@@ -60,6 +117,19 @@
     s_recv,
     a_send,
     a_recv,
+    w_sem,
+    d_send,
+    d_recv,
+    g_send,
+    g_recv,
+    c_send,
+    c_recv,
+    h_send,
+    h_recv,
+    f_send,
+    f_recv,
+    r_send,
+    r_recv,
 ):
     sp = lax.axis_index("sp")
     tp = lax.axis_index("tp")
@@ -74,6 +144,9 @@
 
     def along_tp(k):
         return (sp, lax.rem(tp + k, heads))
+
+    def expert_at(dz, dx):
+        return lax.rem(z + dz, Z_RING) * X_RING + lax.rem(x + dx, X_RING)
 
     own_q = QPLACE[0] * tok
     loads = [
@@ -92,12 +165,22 @@
     for c in loads:
         c.start()
 
+    weights = [
+        pltpu.make_async_copy(src, dst, w_sem.at[i])
+        for i, (src, dst) in enumerate(
+            (
+                (out_narrow, mix_narrow),
+                (out_wide, mix_wide),
+                (gate_proj.at[0], gate),
+                (up_proj.at[0], up),
+                (down_proj.at[0], down),
+            )
+        )
+    ]
+    others = [(dz, dx) for dz in STEPS_Z for dx in range(X_RING) if dz or dx]
     barrier = pltpu.get_barrier_semaphore()
-    peers = (
-        [along_z(1), along_z(Z_RING - 1)]
-        + [along_x(k) for k in range(1, X_RING)]
-        + [along_tp(k) for k in range(1, heads)]
-    )
+    peers = [(expert_at(dz, dx), tp) for dz, dx in others]
+    peers = peers + [along_tp(k) for k in range(1, heads)]
     for peer in peers:
         pl.semaphore_signal(barrier, inc=1, device_id=peer, device_id_type=MESH)
     keys[:, 0:128] = jnp.ones((keys.shape[0], 128), jnp.bfloat16)
@@ -114,6 +197,26 @@
             src_ref=src, dst_ref=dst, send_sem=send, recv_sem=recv, device_id=peer,
             device_id_type=MESH,
         )
+
+    local_rows, top_count = expert_ids.shape
+    experts = Z_RING * X_RING
+
+    def choose():
+        lane = lax.broadcasted_iota(jnp.int32, (local_rows, experts), 1)
+        named = [(expert_ids[:, c : c + 1] == lane).astype(jnp.float32) for c in range(top_count)]
+        i = lax.broadcasted_iota(jnp.int32, (local_rows, local_rows), 0)
+        j = lax.broadcasted_iota(jnp.int32, (local_rows, local_rows), 1)
+        earlier = (j < i).astype(jnp.float32).astype(jnp.bfloat16)
+        before = jnp.dot(
+            earlier, functools.reduce(jnp.add, named).astype(jnp.bfloat16),
+            preferred_element_type=jnp.float32,
+        )
+        row = lax.broadcasted_iota(jnp.int32, (local_rows, experts * capacity), 1)
+        for c in range(top_count):
+            position = jnp.sum(before * named[c], -1, keepdims=True)
+            slot = expert_ids[:, c : c + 1].astype(jnp.float32) * capacity + position
+            picks[c] = (slot == row.astype(jnp.float32)).astype(jnp.float32).astype(jnp.bfloat16)
+            before = before + named[c]
 
     def ring_copy(way, step, piece):
         cols = WIDE if piece else NARROW
@@ -160,6 +263,9 @@
     for k in (1, 3, 2):
         query_copies[k].start()
     start_step(1, 1)
+    for c in weights:
+        c.start()
+    choose()
 
     pair = 2 * tok
 
@@ -249,7 +355,7 @@
         peak = functools.reduce(jnp.maximum, lse)
         weight = [jnp.exp2(v - peak) for v in lse]
         row = lax.broadcasted_iota(jnp.int32, peak.shape, 0)
-        factor = jnp.where(row == 1, -subtract[head], 1.0) / functools.reduce(jnp.add, weight)
+        factor = jnp.where(row == 1, -(subtract_wide if head else subtract_narrow)[0], 1.0) / functools.reduce(jnp.add, weight)
         wide = jnp.concatenate(
             [w * factor for w in weight]
             + [jnp.zeros((128 - 8 * X_RING, peak.shape[1]), jnp.float32)],
@@ -305,197 +411,39 @@
 
     def head_copy(k):
         return remote(
-            attended.at[lax.rem(tp + k, heads)], gathered.at[tp], a_send.at[k], a_recv.at[k],
+            attended.at[lax.rem(tp + k, heads)], gathered_heads.at[tp], a_send.at[k], a_recv.at[k],
             along_tp(k),
         )
 
     for k in range(1, heads):
         head_copy(k).start()
-    gathered[pl.ds(tp, 1)] = attended[pl.ds(tp, 1)]
+    gathered_heads[pl.ds(tp, 1)] = attended[pl.ds(tp, 1)]
     for k in range(1, heads):
         head_copy(k).wait_recv()
-    out[...] = gathered[...]
-    for c in ring.values():
-        c.wait_send()
-    for c in query_copies.values():
-        c.wait_send()
-    for head in range(2):
-        for k in range(1, X_RING):
-            for c in share_copy(head, k):
-                c.wait_send()
-    for k in range(1, heads):
-        head_copy(k).wait_send()
-
-
-def attend(
-    query_narrow, key_narrow, value_narrow, query_wide, key_wide, value_wide, subtract_narrow,
-    subtract_wide, head_gain,
-):
-    tok = query_narrow.shape[0]
-    heads = lax.axis_size("tp")
-    lanes = (tok + 127) // 128 * 128
-    vmem = pl.BlockSpec(memory_space=pltpu.VMEM)
-    hbm = pl.BlockSpec(memory_space=pl.ANY)
-    dma = pltpu.SemaphoreType.DMA
-    bf16, f32 = jnp.bfloat16, jnp.float32
-    return pl.pallas_call(
-        functools.partial(attend_kernel, tok),
-        out_shape=jax.ShapeDtypeStruct((heads, tok // heads, 256), bf16),
-        in_specs=[hbm] * 6 + [pl.BlockSpec(memory_space=pltpu.SMEM), vmem],
-        out_specs=vmem,
-        scratch_shapes=[
-            pltpu.VMEM((X_RING * tok, 384), bf16),
-            pltpu.VMEM((Z_RING * tok, ROW), bf16),
-            pltpu.VMEM((4, X_RING * tok, 128), f32),
-            pltpu.VMEM((4, X_RING * tok, 256), f32),
-            pltpu.VMEM((lanes, 128), f32),
-            pltpu.VMEM((2 * X_RING, tok, 256), bf16),
-            pltpu.VMEM((2 * X_RING, 8, lanes), f32),
-            pltpu.VMEM((2 * X_RING, tok, 256), bf16),
-            pltpu.VMEM((2 * X_RING, 8, lanes), f32),
-            pltpu.VMEM((heads, tok // heads, 256), bf16),
-            pltpu.VMEM((heads, tok // heads, 256), bf16),
-            dma((6,)),
-            dma((X_RING,)),
-            dma((X_RING,)),
-            dma((2 * Z_RING,)),
-            dma((2 * Z_RING,)),
-            dma((2 * X_RING,)),
-            dma((2 * X_RING,)),
-            dma((2 * X_RING,)),
-            dma((2 * X_RING,)),
-            dma((heads,)),
-            dma((heads,)),
-        ],
-        compiler_params=pltpu.CompilerParams(
-            collective_id=0, has_side_effects=True, vmem_limit_bytes=56 * 1024 * 1024
-        ),
-        name="attend",
-    )(
-        query_narrow, key_narrow, value_narrow, query_wide, key_wide, value_wide,
-        jnp.concatenate([subtract_narrow, subtract_wide]), head_gain.reshape(1, -1),
-    )
-
-
-def mixed_heads(attended, out_narrow, out_wide):
-    rows = attended.shape[1]
-    turned = jnp.transpose(attended, (1, 0, 2))
-    narrow = turned[:, :, :128].reshape(rows, -1)
-    wide = turned[:, :, 128:].reshape(rows, -1)
-    return jnp.dot(narrow, out_narrow, preferred_element_type=jnp.float32) + jnp.dot(
-        wide, out_wide, preferred_element_type=jnp.float32
-    )
-
-
-Y_RING = 4
-STEPS_Z = (0, 1, 7, 4, 2, 6, 3, 5)
-GROUPS = 2
-LANES = 128
-
-
-def to_tiles(values, words, target, first):
-    rows, width = values.shape
-    tall = width // LANES
-    for j in range(tall):
-        words[pl.ds(j, rows, stride=tall), :] = values[:, LANES * j : LANES * (j + 1)]
-    flat = words[0 : rows * tall, :]
-    target[first : first + rows] = flat.reshape(rows, tall, LANES).astype(jnp.bfloat16)
-
-
-def from_tiles(source, first, rows, words, target):
-    tall = source.shape[1]
-    flat = source[first : first + rows].astype(jnp.float32)
-    words[0 : rows * tall, :] = flat.reshape(rows * tall, LANES)
-    for j in range(tall):
-        target[:, LANES * j : LANES * (j + 1)] = words[pl.ds(j, rows, stride=tall), :].astype(
-            jnp.bfloat16
-        )
-
-
-def experts_kernel(
-    capacity,
-    hidden,
-    slots_across,
-    slots_down,
-    expert_weight,
-    norm2_gain,
-    gate_proj,
-    up_proj,
-    down_proj,
-    out,
-    gate,
-    up,
-    down,
-    words,
-    outgoing,
-    received,
-    gathered,
-    partial,
-    from_core,
-    half_sum,
-    from_half,
-    whole_sum,
-    from_side,
-    results,
-    returned,
-    returned_rows,
-    w_sem,
-    d_send,
-    d_recv,
-    g_send,
-    g_recv,
-    c_send,
-    c_recv,
-    h_send,
-    h_recv,
-    f_send,
-    f_recv,
-    r_send,
-    r_recv,
-):
-    sp = lax.axis_index("sp")
-    tp = lax.axis_index("tp")
-    z, x = sp // X_RING, sp % X_RING
+    weights[0].wait()
+    weights[1].wait()
+    narrow = jnp.concatenate([gathered_heads[t, :, 0:128] for t in range(8)], 1)
+    wide = jnp.concatenate([gathered_heads[t, :, 128:256] for t in range(8)], 1)
+    mix = jnp.dot(narrow, mix_narrow[...], preferred_element_type=jnp.float32)
+    mix = mix + jnp.dot(wide, mix_wide[...], preferred_element_type=jnp.float32)
+    hidden[...] = layer_norm(
+        residual_scale * residual[...].astype(jnp.float32) + mix, norm1_gain[...]
+    ).astype(jnp.bfloat16)
+
     y, core = tp // 2, tp % 2
-    experts = Z_RING * X_RING
     width = hidden.shape[1]
     half = width // 2
     f32, bf16 = jnp.float32, jnp.bfloat16
 
-    def expert_at(dz, dx):
-        return lax.rem(z + dz, Z_RING) * X_RING + lax.rem(x + dx, X_RING)
-
     def along_y(k):
         return (sp, lax.rem(y + k, Y_RING) * 2 + core)
 
     sibling = (sp, y * 2 + 1 - core)
-    loads = [
-        pltpu.make_async_copy(src.at[0], dst, w_sem.at[i])
-        for i, (src, dst) in enumerate(((gate_proj, gate), (up_proj, up), (down_proj, down)))
-    ]
-    for c in loads:
-        c.start()
-    others = [(dz, dx) for dz in STEPS_Z for dx in range(X_RING) if dz or dx]
-    peers = [(expert_at(dz, dx), tp) for dz, dx in others]
-    peers = peers + [sibling, along_y(1), along_y(Y_RING - 1)]
-    barrier = pltpu.get_barrier_semaphore()
-    for peer in peers:
-        pl.semaphore_signal(barrier, inc=1, device_id=peer, device_id_type=MESH)
-
-    local_rows, top_count = expert_weight.shape
-    row = lax.broadcasted_iota(jnp.int32, (experts * capacity, local_rows), 0)
-    table = jnp.zeros(row.shape, f32)
-    for c in range(top_count):
-        table = jnp.where(row == slots_across[c : c + 1, :], 1.0, table)
-    rows = jnp.dot(table.astype(bf16), hidden[...], preferred_element_type=f32)
+    table = functools.reduce(jnp.add, [picks[c] for c in range(top_count)])
+    rows = lax.dot_general(
+        table, hidden[...], (((0,), (0,)), ((), ())), preferred_element_type=f32
+    )
     to_tiles(rows, words, outgoing, 0)
-    pl.semaphore_wait(barrier, len(peers))
-
-    def remote(src, dst, send, recv, peer):
-        return pltpu.make_async_remote_copy(
-            src_ref=src, dst_ref=dst, send_sem=send, recv_sem=recv, device_id=peer,
-            device_id_type=MESH,
-        )
 
     def place(dz, dx):
         return STEPS_Z.index(dz % Z_RING) * X_RING + dx % X_RING
@@ -654,7 +602,7 @@
     pass_on(0)
     open_group(1)
     close_gather(0)
-    for c in loads:
+    for c in weights[2:]:
         c.wait()
     multiply(0)
     pass_on(1)
@@ -669,11 +617,9 @@
     for dz, dx in others:
         return_copy(-dz % Z_RING, -dx % X_RING).wait_recv()
     from_tiles(returned, 0, experts * capacity, words, returned_rows)
-    column = lax.broadcasted_iota(jnp.int32, (local_rows, experts * capacity), 1)
     routed = jnp.zeros((local_rows, width), f32)
     for c in range(top_count):
-        pick = (column == slots_down[:, c : c + 1]).astype(f32).astype(bf16)
-        picked = jnp.dot(pick, returned_rows[...], preferred_element_type=f32)
+        picked = jnp.dot(picks[c], returned_rows[...], preferred_element_type=f32)
         routed = routed + expert_weight[:, c : c + 1] * picked
     out[...] = layer_norm(
         residual_scale * hidden[...].astype(f32) + routed, norm2_gain[...]
@@ -690,63 +636,16 @@
             half_copy(g, way).wait_send()
             for part in range(2):
                 side_copy(g, way, part).wait_send()
-
-
-def run_experts(hidden, slots, capacity, expert_weight, norm2_gain, gate_proj, up_proj, down_proj):
-    local_rows, width = hidden.shape
-    experts = Z_RING * X_RING
-    inner = gate_proj.shape[2]
-    count = experts * capacity
-    block = count // GROUPS
-    tall = width // LANES
-    vmem = pl.BlockSpec(memory_space=pltpu.VMEM)
-    hbm = pl.BlockSpec(memory_space=pl.ANY)
-    dma = pltpu.SemaphoreType.DMA
-    bf16, f32 = jnp.bfloat16, jnp.float32
-    return pl.pallas_call(
-        functools.partial(experts_kernel, capacity),
-        out_shape=jax.ShapeDtypeStruct((local_rows, width), bf16),
-        in_specs=[vmem] * 5 + [hbm] * 3,
-        out_specs=vmem,
-        scratch_shapes=[
-            pltpu.VMEM((width, inner), bf16),
-            pltpu.VMEM((width, inner), bf16),
-            pltpu.VMEM((inner, width), bf16),
-            pltpu.VMEM((count * tall, LANES), f32),
-            pltpu.VMEM((count, tall, LANES), bf16),
-            pltpu.VMEM((count, tall, LANES), bf16),
-            pltpu.VMEM((GROUPS, 2 * Y_RING, block, width), bf16),
-            pltpu.VMEM((GROUPS, 2 * Y_RING, block, width), bf16),
-            pltpu.VMEM((GROUPS, Y_RING, block, width), bf16),
-            pltpu.VMEM((GROUPS, 2, block, width // 2), bf16),
-            pltpu.VMEM((GROUPS, 2, block, width // 2), bf16),
-            pltpu.VMEM((GROUPS, 2, block, width), bf16),
-            pltpu.VMEM((GROUPS, 2, block, width), bf16),
-            pltpu.VMEM((count, tall, LANES), bf16),
-            pltpu.VMEM((count, tall, LANES), bf16),
-            pltpu.VMEM((count, width), bf16),
-            dma((3,)),
-            dma((experts,)),
-            dma((experts,)),
-            dma((GROUPS, 8)),
-            dma((GROUPS, 8)),
-            dma((GROUPS, Y_RING)),
-            dma((GROUPS, Y_RING)),
-            dma((GROUPS, 2)),
-            dma((GROUPS, 2)),
-            dma((GROUPS, 2, 2)),
-            dma((GROUPS, 2, 2)),
-            dma((experts,)),
-            dma((experts,)),
-        ],
-        compiler_params=pltpu.CompilerParams(
-            collective_id=1, has_side_effects=True, vmem_limit_bytes=56 * 1024 * 1024
-        ),
-        name="experts",
-    )(
-        hidden, jnp.transpose(slots), slots, expert_weight, norm2_gain.reshape(1, -1), gate_proj,
-        up_proj, down_proj,
-    )
+    for c in ring.values():
+        c.wait_send()
+    for c in query_copies.values():
+        c.wait_send()
+    for head in range(2):
+        for k in range(1, X_RING):
+            for c in share_copy(head, k):
+                c.wait_send()
+    for k in range(1, heads):
+        head_copy(k).wait_send()
 
 
 def on_device(
@@ -770,24 +669,92 @@
     up_proj,
     down_proj,
 ):
-    attended = attend(
-        query_narrow, key_narrow, value_narrow, query_wide, key_wide, value_wide,
-        subtract_narrow, subtract_wide, head_gain,
-    )
-    mix = mixed_heads(attended, out_narrow, out_wide)
-    hidden = layer_norm(residual_scale * residual.astype(jnp.float32) + mix, norm1_gain).astype(
-        jnp.bfloat16
-    )
-    local_rows, top_count = expert_ids.shape
-    experts = lax.axis_size("sp")
-    capacity = max(2, 3 * local_rows * top_count // (2 * experts))
-    flat_ids = expert_ids.reshape(-1)
-    onehot = (flat_ids[:, None] == jnp.arange(experts, dtype=jnp.int32)[None, :]).astype(jnp.int32)
-    before = jnp.cumsum(onehot, 0) - onehot
-    position = jnp.sum(before * onehot, 1)
-    slots = (flat_ids * capacity + position).reshape(local_rows, top_count)
-    return run_experts(
-        hidden, slots, capacity, expert_weight, norm2_gain, gate_proj, up_proj, down_proj
+    tok = query_narrow.shape[0]
+    heads = lax.axis_size("tp")
+    lanes = (tok + 127) // 128 * 128
+    local_rows, width = residual.shape
+    experts = Z_RING * X_RING
+    capacity = max(2, 3 * local_rows * expert_ids.shape[1] // (2 * experts))
+    inner = gate_proj.shape[2]
+    count = experts * capacity
+    block = count // GROUPS
+    tall = width // LANES
+    vmem = pl.BlockSpec(memory_space=pltpu.VMEM)
+    smem = pl.BlockSpec(memory_space=pltpu.SMEM)
+    hbm = pl.BlockSpec(memory_space=pl.ANY)
+    dma = pltpu.SemaphoreType.DMA
+    bf16, f32 = jnp.bfloat16, jnp.float32
+    return pl.pallas_call(
+        functools.partial(layer_kernel, tok, capacity),
+        out_shape=jax.ShapeDtypeStruct((local_rows, width), bf16),
+        in_specs=[vmem] + [hbm] * 6 + [smem] * 2 + [vmem] + [hbm] * 2 + [vmem] * 4 + [hbm] * 3,
+        out_specs=vmem,
+        scratch_shapes=[
+            pltpu.VMEM((X_RING * tok, 384), bf16),
+            pltpu.VMEM((Z_RING * tok, ROW), bf16),
+            pltpu.VMEM((4, X_RING * tok, 128), f32),
+            pltpu.VMEM((4, X_RING * tok, 256), f32),
+            pltpu.VMEM((lanes, 128), f32),
+            pltpu.VMEM((2 * X_RING, tok, 256), bf16),
+            pltpu.VMEM((2 * X_RING, 8, lanes), f32),
+            pltpu.VMEM((2 * X_RING, tok, 256), bf16),
+            pltpu.VMEM((2 * X_RING, 8, lanes), f32),
+            pltpu.VMEM((heads, tok // heads, 256), bf16),
+            pltpu.VMEM((heads, tok // heads, 256), bf16),
+            pltpu.VMEM(out_narrow.shape, bf16),
+            pltpu.VMEM(out_wide.shape, bf16),
+            pltpu.VMEM(residual.shape, bf16),
+            pltpu.VMEM((expert_ids.shape[1], local_rows, count), bf16),
+            pltpu.VMEM((width, inner), bf16),
+            pltpu.VMEM((width, inner), bf16),
+            pltpu.VMEM((inner, width), bf16),
+            pltpu.VMEM((count * tall, LANES), f32),
+            pltpu.VMEM((count, tall, LANES), bf16),
+            pltpu.VMEM((count, tall, LANES), bf16),
+            pltpu.VMEM((GROUPS, 2 * Y_RING, block, width), bf16),
+            pltpu.VMEM((GROUPS, 2 * Y_RING, block, width), bf16),
+            pltpu.VMEM((GROUPS, Y_RING, block, width), bf16),
+            pltpu.VMEM((GROUPS, 2, block, width // 2), bf16),
+            pltpu.VMEM((GROUPS, 2, block, width // 2), bf16),
+            pltpu.VMEM((GROUPS, 2, block, width), bf16),
+            pltpu.VMEM((GROUPS, 2, block, width), bf16),
+            pltpu.VMEM((count, tall, LANES), bf16),
+            pltpu.VMEM((count, tall, LANES), bf16),
+            pltpu.VMEM((count, width), bf16),
+            dma((6,)),
+            dma((X_RING,)),
+            dma((X_RING,)),
+            dma((2 * Z_RING,)),
+            dma((2 * Z_RING,)),
+            dma((2 * X_RING,)),
+            dma((2 * X_RING,)),
+            dma((2 * X_RING,)),
+            dma((2 * X_RING,)),
+            dma((heads,)),
+            dma((heads,)),
+            dma((5,)),
+            dma((experts,)),
+            dma((experts,)),
+            dma((GROUPS, 8)),
+            dma((GROUPS, 8)),
+            dma((GROUPS, Y_RING)),
+            dma((GROUPS, Y_RING)),
+            dma((GROUPS, 2)),
+            dma((GROUPS, 2)),
+            dma((GROUPS, 2, 2)),
+            dma((GROUPS, 2, 2)),
+            dma((experts,)),
+            dma((experts,)),
+        ],
+        compiler_params=pltpu.CompilerParams(
+            collective_id=0, has_side_effects=True, vmem_limit_bytes=66 * 1000 * 1000
+        ),
+        name="layer",
+    )(
+        residual, query_narrow, key_narrow, value_narrow, query_wide, key_wide, value_wide,
+        subtract_narrow, subtract_wide, head_gain.reshape(1, -1), out_narrow, out_wide,
+        norm1_gain.reshape(1, -1), norm2_gain.reshape(1, -1), expert_ids, expert_weight,
+        gate_proj, up_proj, down_proj,
     )
 
 

time: 139 us -> 130 us (0.935)
  matrix products: 3.98 us -> 0 us
  Pallas kernels: 125 us -> 122 us
  other arithmetic: 1.97 us -> 0 us
    dot_general x2 -> x0, matrix products: 3.98 us -> none  [the longest x1 3.02 us: mixed_heads(): jnp.dot(narrow, out_narrow, preferred_element_type=jnp.float32)]
    pallas_call x2 -> x1, Pallas kernels: 125 us -> 122 us  [on_device(): pl.pallas_call(functools.partial(layer_kernel, tok, capacity), out_shape=...]
    unnamed x16 -> x3, local copies, waits for them, and re-layouts: 3.35 us -> 4.32 us
where the time goes in v3:
time: 130 us; the launch traced here: 128 us
  Pallas kernels  122 us (94%)
  local copies, waits for them, and re-layouts  4.32 us (3%)
  between operations  1.31 us (1%)
    pallas_call x1, Pallas kernels, on_device(): pl.pallas_call(functools.partial(layer_kernel, tok, capacity), out_shape=...  122 us
    unnamed x3, local copies, waits for them, and re-layouts  4.32 us

profile of v3, /device:TPU:2, one launch (start us, length us, event | category | flops | bytes accessed | tf_op | source)
XLA Modules:
  0.0 127.9 jit_solution(9476338256648246959)
XLA Ops:
  1.3 1.4 %copy.20.expert_ids = s32[40,2]{1,0:T(8,128)} copy(s32[40,2]{0,1:T(2,128)} %param.33) | data formatting | bytes 640 | tf_op args[14]
  2.7 1.4 %copy.21.expert_weight = f32[40,2]{1,0:T(8,128)} copy(f32[40,2]{0,1:T(2,128)} %param.34) | data formatting | bytes 640 | tf_op args[15]
  4.0 122.3 %layer.1 = bf16[40,2048]{1,0:T(8,128)(2,1)} custom-call(bf16[40,2048]{1,0:T(8,128)(2,1)} %residual.1, bf16[320,128]{1,0:T(8,128)(2,1)} %query_narrow.1, bf16[320,128]{1,0:T(8,128)(2,1)} %key_narrow.1, bf16[320,128]{1,0:T(8,128)(2,1)} %value_narrow.1, bf16[320,256]{1,0:T(8,128)(2,1)} %query_wide.1, bf16[320,256]{1,0:T(8,128)(2,1)} %key_wide.1, ...), custom_call_target="tpu_custom_call" | custom-call | tf_op jit(solution)/shard_map/layer/pallas_call | solution.py:687
  126.3 1.6 %copy.25 = bf16[40,2048]{1,0:T(8,128)(2,1)} copy(bf16[40,2048]{1,0:T(8,128)(2,1)} %layer.1) | data formatting | bytes 327680

commit v4 on v3

--- a/solution.py
+++ b/solution.py
@@ -28,8 +28,6 @@
 
 
 Y_RING = 4
-STEPS_Z = (0, 1, 7, 4, 2, 6, 3, 5)
-GROUPS = 2
 LANES = 128
 
 
@@ -90,6 +88,7 @@
     mix_wide,
     hidden,
     picks,
+    scales,
     gate,
     up,
     down,
@@ -177,9 +176,9 @@
             )
         )
     ]
-    others = [(dz, dx) for dz in STEPS_Z for dx in range(X_RING) if dz or dx]
+    others = [(dz, dx) for dz in (4, 3, 5, 2, 6, 1, 7, 0) for dx in range(X_RING) if dz or dx]
     barrier = pltpu.get_barrier_semaphore()
-    peers = [(expert_at(dz, dx), tp) for dz, dx in others]
+    peers = [along_z(1), along_z(Z_RING - 1)] + [along_x(k) for k in range(1, X_RING)]
     peers = peers + [along_tp(k) for k in range(1, heads)]
     for peer in peers:
         pl.semaphore_signal(barrier, inc=1, device_id=peer, device_id_type=MESH)
@@ -198,25 +197,27 @@
             device_id_type=MESH,
         )
 
-    local_rows, top_count = expert_ids.shape
+    top_count, local_rows = expert_ids.shape
     experts = Z_RING * X_RING
 
     def choose():
-        lane = lax.broadcasted_iota(jnp.int32, (local_rows, experts), 1)
-        named = [(expert_ids[:, c : c + 1] == lane).astype(jnp.float32) for c in range(top_count)]
+        lane = lax.broadcasted_iota(jnp.int32, (experts, local_rows), 0)
+        named = [(expert_ids[c : c + 1, :] == lane).astype(jnp.float32) for c in range(top_count)]
         i = lax.broadcasted_iota(jnp.int32, (local_rows, local_rows), 0)
         j = lax.broadcasted_iota(jnp.int32, (local_rows, local_rows), 1)
-        earlier = (j < i).astype(jnp.float32).astype(jnp.bfloat16)
+        earlier = (i < j).astype(jnp.float32).astype(jnp.bfloat16)
         before = jnp.dot(
-            earlier, functools.reduce(jnp.add, named).astype(jnp.bfloat16),
+            functools.reduce(jnp.add, named).astype(jnp.bfloat16), earlier,
             preferred_element_type=jnp.float32,
         )
-        row = lax.broadcasted_iota(jnp.int32, (local_rows, experts * capacity), 1)
+        row = lax.broadcasted_iota(jnp.int32, (experts * capacity, local_rows), 0)
         for c in range(top_count):
-            position = jnp.sum(before * named[c], -1, keepdims=True)
-            slot = expert_ids[:, c : c + 1].astype(jnp.float32) * capacity + position
+            position = jnp.sum(before * named[c], 0, keepdims=True)
+            slot = position * experts + expert_ids[c : c + 1, :].astype(jnp.float32)
             picks[c] = (slot == row.astype(jnp.float32)).astype(jnp.float32).astype(jnp.bfloat16)
             before = before + named[c]
+            own = jnp.where(i == j, expert_weight[c : c + 1, :], 0.0)
+            scales[c] = jnp.broadcast_to(jnp.sum(own, 1, keepdims=True), scales.shape[1:])
 
     def ring_copy(way, step, piece):
         cols = WIDE if piece else NARROW
@@ -375,28 +376,29 @@
 
     arrived(1, 0)
     start_step(2, 0)
+    query_copies[3].wait_recv()
     query_copies[1].wait_recv()
-    absorb(0, 1, 0, 256)
-    absorb(1, 1, 0, 256)
-    query_copies[3].wait_recv()
-    query_copies[2].wait_recv()
-    absorb(0, 0, 0, 256)
-    absorb(1, 0, 0, 256)
+    for head in range(2):
+        absorb(head, 1, 0, 256)
     arrived(1, 1)
     start_step(2, 1)
-    absorb_both(0, 256, 512)
-    absorb_both(1, 256, 512)
+    for head in range(2):
+        absorb(head, 1, 256, 512)
     arrived(2, 0)
     start_step(3, 0)
-    absorb_both(0, 768, 768)
+    query_copies[2].wait_recv()
+    for head in range(2):
+        absorb(head, 0, 0, 768)
     arrived(2, 1)
     start_step(3, 1)
-    absorb_both(1, 768, 768)
+    absorb_both(0, 768, 768)
     arrived(3, 0)
     start_step(4, 0)
-    absorb_both(0, 1536, 512)
+    absorb_both(1, 768, 768)
+    absorb(0, 0, 1536, 512)
     arrived(3, 1)
     start_step(4, 1)
+    absorb(0, 1, 1536, 512)
     absorb_both(1, 1536, 512)
     for head in range(2):
         arrived(4, head)
@@ -440,41 +442,33 @@
 
     sibling = (sp, y * 2 + 1 - core)
     table = functools.reduce(jnp.add, [picks[c] for c in range(top_count)])
-    rows = lax.dot_general(
-        table, hidden[...], (((0,), (0,)), ((), ())), preferred_element_type=f32
-    )
+    rows = jnp.dot(table, hidden[...], preferred_element_type=f32)
     to_tiles(rows, words, outgoing, 0)
 
     def place(dz, dx):
-        return STEPS_Z.index(dz % Z_RING) * X_RING + dx % X_RING
-
-    def dispatch_copy(dz, dx):
+        return dz % Z_RING * X_RING + dx % X_RING
+
+    def dispatch_copy(g, dz, dx):
         e = expert_at(dz, dx)
         p = place(-dz, -dx)
         return remote(
-            outgoing.at[pl.ds(e * capacity, capacity)],
-            received.at[pl.ds(p * capacity, capacity)],
-            d_send.at[p], d_recv.at[p], (e, tp),
-        )
-
-    def return_copy(dz, dx):
+            outgoing.at[g * experts + e], received.at[g * experts + p],
+            d_send.at[g, p], d_recv.at[g, p], (e, tp),
+        )
+
+    def return_copy(g, dz, dx):
         p = place(dz, dx)
         return remote(
-            results.at[pl.ds(p * capacity, capacity)],
-            returned.at[pl.ds(sp * capacity, capacity)],
-            r_send.at[p], r_recv.at[p], (expert_at(dz, dx), tp),
-        )
-
-    per_group = len(STEPS_Z) // GROUPS
-    steps_of = [STEPS_Z[g * per_group : (g + 1) * per_group] for g in range(GROUPS)]
-    hops = [[(dz, dx) for dz in steps_of[g] for dx in range(X_RING)] for g in range(GROUPS)]
-    block = per_group * X_RING * capacity
+            results.at[g * experts + p], returned.at[g * experts + sp],
+            r_send.at[g, p], r_recv.at[g, p], (expert_at(dz, dx), tp),
+        )
+
+    block = experts
     low, high = pl.ds(0, half), pl.ds(half, half)
 
-    for g in range(GROUPS):
-        for dz, dx in hops[g]:
-            if dz or dx:
-                dispatch_copy(dz, dx).start()
+    for g in range(capacity):
+        for dz, dx in others:
+            dispatch_copy(g, dz, dx).start()
 
     def gather_copies(g):
         at = lambda s, c=None: gathered.at[g, s] if c is None else gathered.at[g, s, :, c]
@@ -494,7 +488,7 @@
             for i, (name, (src, dst, peer)) in enumerate(plan.items())
         }
 
-    gathers = [gather_copies(g) for g in range(GROUPS)]
+    gathers = [gather_copies(g) for g in range(capacity)]
 
     def core_copy(g, k):
         return remote(
@@ -515,14 +509,9 @@
         )
 
     def open_group(g):
-        for dz, dx in hops[g]:
-            p = place(dz, dx)
-            if dz or dx:
-                dispatch_copy(-dz % Z_RING, -dx % X_RING).wait_recv()
-            else:
-                received[p * capacity : (p + 1) * capacity] = outgoing[
-                    pl.ds(sp * capacity, capacity)
-                ]
+        received[g * experts] = outgoing[g * experts + sp]
+        for dz, dx in others:
+            dispatch_copy(g, -dz % Z_RING, -dx % X_RING).wait_recv()
         from_tiles(received, g * block, block, words, gathered.at[g, 0])
         for name in ("right", "left", "core0"):
             gathers[g][name].start()
@@ -589,45 +578,50 @@
             + from_side[g, 1].astype(f32)
         )
         to_tiles(total, words, results, g * block)
-        for dz, dx in hops[g]:
-            p = place(dz, dx)
-            if dz or dx:
-                return_copy(dz, dx).start()
-            else:
-                returned[pl.ds(sp * capacity, capacity)] = results[
-                    p * capacity : (p + 1) * capacity
-                ]
+        for dz, dx in others:
+            return_copy(g, dz, dx).start()
+        returned[g * experts + sp] = results[g * experts]
 
     open_group(0)
+    open_group(1)
     pass_on(0)
-    open_group(1)
-    close_gather(0)
+    open_group(2)
+    pass_on(1)
     for c in weights[2:]:
         c.wait()
+    close_gather(0)
     multiply(0)
-    pass_on(1)
+    pass_on(2)
     send_halves(0)
     close_gather(1)
     multiply(1)
     send_sides(0)
     send_halves(1)
+    close_gather(2)
+    multiply(2)
     give_back(0)
     send_sides(1)
+    send_halves(2)
     give_back(1)
-    for dz, dx in others:
-        return_copy(-dz % Z_RING, -dx % X_RING).wait_recv()
+    send_sides(2)
+    give_back(2)
+    for g in range(capacity):
+        for dz, dx in others:
+            return_copy(g, -dz % Z_RING, -dx % X_RING).wait_recv()
     from_tiles(returned, 0, experts * capacity, words, returned_rows)
     routed = jnp.zeros((local_rows, width), f32)
     for c in range(top_count):
-        picked = jnp.dot(picks[c], returned_rows[...], preferred_element_type=f32)
-        routed = routed + expert_weight[:, c : c + 1] * picked
+        picked = lax.dot_general(
+            picks[c], returned_rows[...], (((0,), (0,)), ((), ())), preferred_element_type=f32
+        )
+        routed = routed + scales[c, :, 0:1] * picked
     out[...] = layer_norm(
         residual_scale * hidden[...].astype(f32) + routed, norm2_gain[...]
     ).astype(bf16)
-    for dz, dx in others:
-        dispatch_copy(dz, dx).wait_send()
-        return_copy(dz, dx).wait_send()
-    for g in range(GROUPS):
+    for g in range(capacity):
+        for dz, dx in others:
+            dispatch_copy(g, dz, dx).wait_send()
+            return_copy(g, dz, dx).wait_send()
         for c in gathers[g].values():
             c.wait_send()
         for k in range(Y_RING):
@@ -677,7 +671,7 @@
     capacity = max(2, 3 * local_rows * expert_ids.shape[1] // (2 * experts))
     inner = gate_proj.shape[2]
     count = experts * capacity
-    block = count // GROUPS
+    block = experts
     tall = width // LANES
     vmem = pl.BlockSpec(memory_space=pltpu.VMEM)
     smem = pl.BlockSpec(memory_space=pltpu.SMEM)
@@ -704,20 +698,21 @@
             pltpu.VMEM(out_narrow.shape, bf16),
             pltpu.VMEM(out_wide.shape, bf16),
             pltpu.VMEM(residual.shape, bf16),
-            pltpu.VMEM((expert_ids.shape[1], local_rows, count), bf16),
+            pltpu.VMEM((expert_ids.shape[1], count, local_rows), bf16),
+            pltpu.VMEM((expert_ids.shape[1], local_rows, LANES), f32),
             pltpu.VMEM((width, inner), bf16),
             pltpu.VMEM((width, inner), bf16),
             pltpu.VMEM((inner, width), bf16),
             pltpu.VMEM((count * tall, LANES), f32),
             pltpu.VMEM((count, tall, LANES), bf16),
             pltpu.VMEM((count, tall, LANES), bf16),
-            pltpu.VMEM((GROUPS, 2 * Y_RING, block, width), bf16),
-            pltpu.VMEM((GROUPS, 2 * Y_RING, block, width), bf16),
-            pltpu.VMEM((GROUPS, Y_RING, block, width), bf16),
-            pltpu.VMEM((GROUPS, 2, block, width // 2), bf16),
-            pltpu.VMEM((GROUPS, 2, block, width // 2), bf16),
-            pltpu.VMEM((GROUPS, 2, block, width), bf16),
-            pltpu.VMEM((GROUPS, 2, block, width), bf16),
+            pltpu.VMEM((capacity, 2 * Y_RING, block, width), bf16),
+            pltpu.VMEM((capacity, 2 * Y_RING, block, width), bf16),
+            pltpu.VMEM((capacity, Y_RING, block, width), bf16),
+            pltpu.VMEM((capacity, 2, block, width // 2), bf16),
+            pltpu.VMEM((capacity, 2, block, width // 2), bf16),
+            pltpu.VMEM((capacity, 2, block, width), bf16),
+            pltpu.VMEM((capacity, 2, block, width), bf16),
             pltpu.VMEM((count, tall, LANES), bf16),
             pltpu.VMEM((count, tall, LANES), bf16),
             pltpu.VMEM((count, width), bf16),
@@ -733,18 +728,18 @@
             dma((heads,)),
             dma((heads,)),
             dma((5,)),
-            dma((experts,)),
-            dma((experts,)),
-            dma((GROUPS, 8)),
-            dma((GROUPS, 8)),
-            dma((GROUPS, Y_RING)),
-            dma((GROUPS, Y_RING)),
-            dma((GROUPS, 2)),
-            dma((GROUPS, 2)),
-            dma((GROUPS, 2, 2)),
-            dma((GROUPS, 2, 2)),
-            dma((experts,)),
-            dma((experts,)),
+            dma((capacity, experts)),
+            dma((capacity, experts)),
+            dma((capacity, 8)),
+            dma((capacity, 8)),
+            dma((capacity, Y_RING)),
+            dma((capacity, Y_RING)),
+            dma((capacity, 2)),
+            dma((capacity, 2)),
+            dma((capacity, 2, 2)),
+            dma((capacity, 2, 2)),
+            dma((capacity, experts)),
+            dma((capacity, experts)),
         ],
         compiler_params=pltpu.CompilerParams(
             collective_id=0, has_side_effects=True, vmem_limit_bytes=66 * 1000 * 1000
@@ -753,8 +748,8 @@
     )(
         residual, query_narrow, key_narrow, value_narrow, query_wide, key_wide, value_wide,
         subtract_narrow, subtract_wide, head_gain.reshape(1, -1), out_narrow, out_wide,
-        norm1_gain.reshape(1, -1), norm2_gain.reshape(1, -1), expert_ids, expert_weight,
-        gate_proj, up_proj, down_proj,
+        norm1_gain.reshape(1, -1), norm2_gain.reshape(1, -1), jnp.transpose(expert_ids),
+        jnp.transpose(expert_weight), gate_proj, up_proj, down_proj,
     )
 
 

time: 130 us -> 122 us (0.938); the launches traced: 128 us -> 122 us
  Pallas kernels: 122 us -> 119 us
  local copies, waits for them, and re-layouts: 4.32 us -> 1.59 us
    pallas_call x1, Pallas kernels: 122 us -> 119 us  [on_device(): pl.pallas_call(functools.partial(layer_kernel, tok, capacity), out_shape=...]
    unnamed x3 -> x1, local copies, waits for them, and re-layouts: 4.32 us -> 1.59 us
where the time goes in v4:
time: 122 us
  Pallas kernels  119 us (98%)
  local copies, waits for them, and re-layouts  1.59 us (1%)
  between operations  1.31 us (1%)
    pallas_call x1, Pallas kernels, on_device(): pl.pallas_call(functools.partial(layer_kernel, tok, capacity), out_shape=...  119 us

profile of v4, /device:TPU:2, one launch (start us, length us, event | category | flops | bytes accessed | tf_op | source)
XLA Modules:
  0.0 121.6 jit_solution(1584986349342306315)
XLA Ops:
  1.3 118.7 %layer.1 = bf16[40,2048]{1,0:T(8,128)(2,1)} custom-call(bf16[40,2048]{1,0:T(8,128)(2,1)} %residual.1, bf16[320,128]{1,0:T(8,128)(2,1)} %query_narrow.1, bf16[320,128]{1,0:T(8,128)(2,1)} %key_narrow.1, bf16[320,128]{1,0:T(8,128)(2,1)} %value_narrow.1, bf16[320,256]{1,0:T(8,128)(2,1)} %query_wide.1, bf16[320,256]{1,0:T(8,128)(2,1)} %key_wide.1, ...), custom_call_target="tpu_custom_call" | custom-call | tf_op jit(solution)/shard_map/layer/pallas_call | solution.py:681
  120.0 1.6 %copy.23 = bf16[40,2048]{1,0:T(8,128)(2,1)} copy(bf16[40,2048]{1,0:T(8,128)(2,1)} %layer.1) | data formatting | bytes 327680

commit v5 on v4

--- a/solution.py
+++ b/solution.py
@@ -225,13 +225,13 @@
         source = (Z_RING - step + 1) % Z_RING if forward else step - 1
         target = (Z_RING - step) % Z_RING if forward else step
         r0, rows = 0, tok
-        if 2 * step == Z_RING:
+        if piece or 2 * step == Z_RING:
             rows = tok // 2
-            r0 = 0 if forward else rows
+            r0 = 0 if forward == (piece < 2) else rows
         at = lambda k: keys.at[
             pl.ds(PLACE[k] * tok + r0, rows), pl.ds(cols[0], cols[1] - cols[0])
         ]
-        n = (way * (Z_RING // 2) + step - 1) * 2 + piece
+        n = (way * (Z_RING // 2) + step - 1) * 3 + piece
         return remote(
             at(source), at(target), kv_send.at[n], kv_recv.at[n],
             along_z(1 if forward else Z_RING - 1),
@@ -248,7 +248,7 @@
         (w, s, p): ring_copy(w, s, p)
         for w in range(2)
         for s in range(1, Z_RING // 2 + 1)
-        for p in range(2)
+        for p in range(3 if 2 * s < Z_RING else 2)
     }
     query_copies = {k: query_copy(k) for k in range(1, X_RING)}
 
@@ -259,6 +259,11 @@
     def arrived(step, piece):
         for w in range(2):
             ring[w, step, piece].wait_recv()
+
+    def pass_on_keys(step, piece):
+        for w in range(2):
+            ring[w, step, piece].wait_recv()
+            ring[w, step + 1, piece].start()
 
     start_step(1, 0)
     for k in (1, 3, 2):
@@ -370,64 +375,70 @@
                 diff = diff + turned[:, 8 * k + m : 8 * k + m + 1] * o[:, 128 * m : 128 * m + 128]
         spread = jnp.mean(diff * diff, -1, keepdims=True)
         normed = diff * lax.rsqrt(spread + 1e-06) * head_gain[...]
-        attended[:, :, 128 * head : 128 * head + 128] = normed.reshape(
-            heads, tok // heads, 128
-        ).astype(jnp.bfloat16)
-
-    arrived(1, 0)
-    start_step(2, 0)
+        attended[head] = normed.reshape(heads, tok // heads, 128).astype(jnp.bfloat16)
+
+    pass_on_keys(1, 0)
+    start_step(1, 2)
     query_copies[3].wait_recv()
     query_copies[1].wait_recv()
-    for head in range(2):
-        absorb(head, 1, 0, 256)
-    arrived(1, 1)
-    start_step(2, 1)
-    for head in range(2):
-        absorb(head, 1, 256, 512)
-    arrived(2, 0)
-    start_step(3, 0)
+    absorb(0, 1, 0, 768)
+    pass_on_keys(2, 0)
+    pass_on_keys(1, 1)
     query_copies[2].wait_recv()
-    for head in range(2):
-        absorb(head, 0, 0, 768)
-    arrived(2, 1)
-    start_step(3, 1)
-    absorb_both(0, 768, 768)
-    arrived(3, 0)
-    start_step(4, 0)
+    absorb(0, 0, 0, 768)
+    arrived(1, 2)
+    absorb_both(1, 0, 768)
+    pass_on_keys(3, 0)
+    start_step(2, 2)
+    absorb(0, 0, 768, 768)
+    pass_on_keys(2, 1)
+    absorb(0, 1, 768, 768)
+    absorb_both(0, 1536, 512)
+    arrived(4, 0)
+    absorb(0, 0, 2048, 512)
+    arrived(2, 2)
+    start_step(3, 2)
+    finish(0, 2)
+    finish(0, 1)
+    absorb(0, 1, 2048, 512)
+    finish(0, 3)
+    pass_on_keys(3, 1)
+    finish(0, 0)
     absorb_both(1, 768, 768)
-    absorb(0, 0, 1536, 512)
-    arrived(3, 1)
-    start_step(4, 1)
-    absorb(0, 1, 1536, 512)
+    arrived(3, 2)
     absorb_both(1, 1536, 512)
-    for head in range(2):
-        arrived(4, head)
-        absorb(head, 0, 2048, 512)
-        finish(head, 2)
-        finish(head, 1)
-        absorb(head, 1, 2048, 512)
-        finish(head, 3)
-        finish(head, 0)
-    for head in range(2):
+    arrived(4, 1)
+    absorb(1, 0, 2048, 512)
+    finish(1, 2)
+    finish(1, 1)
+    absorb(1, 1, 2048, 512)
+    finish(1, 3)
+    finish(1, 0)
+
+    def head_copy(head, k):
+        return remote(
+            attended.at[head, lax.rem(tp + k, heads)], gathered_heads.at[head, tp],
+            a_send.at[head, k], a_recv.at[head, k], along_tp(k),
+        )
+
+    def send_heads(head):
         combine(head)
-
-    def head_copy(k):
-        return remote(
-            attended.at[lax.rem(tp + k, heads)], gathered_heads.at[tp], a_send.at[k], a_recv.at[k],
-            along_tp(k),
-        )
-
-    for k in range(1, heads):
-        head_copy(k).start()
-    gathered_heads[pl.ds(tp, 1)] = attended[pl.ds(tp, 1)]
-    for k in range(1, heads):
-        head_copy(k).wait_recv()
+        for k in range(1, heads):
+            head_copy(head, k).start()
+        gathered_heads[head, pl.ds(tp, 1)] = attended[head, pl.ds(tp, 1)]
+
+    def project(head, weight):
+        for k in range(1, heads):
+            head_copy(head, k).wait_recv()
+        all_heads = jnp.concatenate([gathered_heads[head, t] for t in range(heads)], 1)
+        return jnp.dot(all_heads, weight[...], preferred_element_type=jnp.float32)
+
+    send_heads(0)
     weights[0].wait()
     weights[1].wait()
-    narrow = jnp.concatenate([gathered_heads[t, :, 0:128] for t in range(8)], 1)
-    wide = jnp.concatenate([gathered_heads[t, :, 128:256] for t in range(8)], 1)
-    mix = jnp.dot(narrow, mix_narrow[...], preferred_element_type=jnp.float32)
-    mix = mix + jnp.dot(wide, mix_wide[...], preferred_element_type=jnp.float32)
+    mix = project(0, mix_narrow)
+    send_heads(1)
+    mix = mix + project(1, mix_wide)
     hidden[...] = layer_norm(
         residual_scale * residual[...].astype(jnp.float32) + mix, norm1_gain[...]
     ).astype(jnp.bfloat16)
@@ -638,8 +649,9 @@
         for k in range(1, X_RING):
             for c in share_copy(head, k):
                 c.wait_send()
-    for k in range(1, heads):
-        head_copy(k).wait_send()
+    for head in range(2):
+        for k in range(1, heads):
+            head_copy(head, k).wait_send()
 
 
 def on_device(
@@ -693,8 +705,8 @@
             pltpu.VMEM((2 * X_RING, 8, lanes), f32),
             pltpu.VMEM((2 * X_RING, tok, 256), bf16),
             pltpu.VMEM((2 * X_RING, 8, lanes), f32),
-            pltpu.VMEM((heads, tok // heads, 256), bf16),
-            pltpu.VMEM((heads, tok // heads, 256), bf16),
+            pltpu.VMEM((2, heads, tok // heads, 128), bf16),
+            pltpu.VMEM((2, heads, tok // heads, 128), bf16),
             pltpu.VMEM(out_narrow.shape, bf16),
             pltpu.VMEM(out_wide.shape, bf16),
             pltpu.VMEM(residual.shape, bf16),
@@ -719,14 +731,14 @@
             dma((6,)),
             dma((X_RING,)),
             dma((X_RING,)),
-            dma((2 * Z_RING,)),
-            dma((2 * Z_RING,)),
+            dma((3 * Z_RING,)),
+            dma((3 * Z_RING,)),
             dma((2 * X_RING,)),
             dma((2 * X_RING,)),
             dma((2 * X_RING,)),
             dma((2 * X_RING,)),
-            dma((heads,)),
-            dma((heads,)),
+            dma((2, heads)),
+            dma((2, heads)),
             dma((5,)),
             dma((capacity, experts)),
             dma((capacity, experts)),

time: 122 us -> 116 us (0.951)
  Pallas kernels: 119 us -> 113 us
    pallas_call x1, Pallas kernels: 119 us -> 113 us  [on_device(): pl.pallas_call(functools.partial(layer_kernel, tok, capacity), out_shape=...]
where the time goes in v5:
time: 116 us
  Pallas kernels  113 us (97%)
  local copies, waits for them, and re-layouts  1.59 us (1%)
  between operations  1.31 us (1%)
    pallas_call x1, Pallas kernels, on_device(): pl.pallas_call(functools.partial(layer_kernel, tok, capacity), out_shape=...  113 us

profile of v5, /device:TPU:2, one launch (start us, length us, event | category | flops | bytes accessed | tf_op | source)
XLA Modules:
  0.0 115.8 jit_solution(190584600760695852)
XLA Ops:
  1.3 112.9 %layer.1 = bf16[40,2048]{1,0:T(8,128)(2,1)} custom-call(bf16[40,2048]{1,0:T(8,128)(2,1)} %residual.1, bf16[320,128]{1,0:T(8,128)(2,1)} %query_narrow.1, bf16[320,128]{1,0:T(8,128)(2,1)} %key_narrow.1, bf16[320,128]{1,0:T(8,128)(2,1)} %value_narrow.1, bf16[320,256]{1,0:T(8,128)(2,1)} %query_wide.1, bf16[320,256]{1,0:T(8,128)(2,1)} %key_wide.1, ...), custom_call_target="tpu_custom_call" | custom-call | tf_op jit(solution)/shard_map/layer/pallas_call | solution.py:693
  114.2 1.6 %copy.23 = bf16[40,2048]{1,0:T(8,128)(2,1)} copy(bf16[40,2048]{1,0:T(8,128)(2,1)} %layer.1) | data formatting | bytes 327680

commit v6 on v5

--- a/solution.py
+++ b/solution.py
@@ -423,7 +423,7 @@
 
     def send_heads(head):
         combine(head)
-        for k in range(1, heads):
+        for k in sorted(range(1, heads), key=lambda k: abs(k - heads // 2)):
             head_copy(head, k).start()
         gathered_heads[head, pl.ds(tp, 1)] = attended[head, pl.ds(tp, 1)]
 
@@ -452,10 +452,6 @@
         return (sp, lax.rem(y + k, Y_RING) * 2 + core)
 
     sibling = (sp, y * 2 + 1 - core)
-    table = functools.reduce(jnp.add, [picks[c] for c in range(top_count)])
-    rows = jnp.dot(table, hidden[...], preferred_element_type=f32)
-    to_tiles(rows, words, outgoing, 0)
-
     def place(dz, dx):
         return dz % Z_RING * X_RING + dx % X_RING
 
@@ -478,6 +474,10 @@
     low, high = pl.ds(0, half), pl.ds(half, half)
 
     for g in range(capacity):
+        part = pl.ds(g * experts, experts)
+        table = functools.reduce(jnp.add, [picks[c, part] for c in range(top_count)])
+        rows = jnp.dot(table, hidden[...], preferred_element_type=f32)
+        to_tiles(rows, words, outgoing, g * experts)
         for dz, dx in others:
             dispatch_copy(g, dz, dx).start()
 
@@ -539,18 +539,21 @@
         gathers[g]["right2"].wait_recv()
         gathers[g]["left2"].wait_recv()
         gathers[g]["core2"].start()
+        multiply(g, (0, 2, 4, 6))
         for name in ("core0", "core1", "core3", "core2"):
             gathers[g][name].wait_recv()
-
-    def multiply(g):
-        flat = gathered[g].reshape(-1, width)
+        multiply(g, (5, 3, 7, 1))
+
+    def multiply(g, slots):
+        flat = jnp.concatenate([gathered[g, n] for n in slots], 0)
         gate_part = jnp.dot(flat, gate[...], preferred_element_type=f32)
         up_part = jnp.dot(flat, up[...], preferred_element_type=f32)
         inner = (gate_part * jax.nn.sigmoid(gate_part) * up_part).astype(bf16)
         share = jnp.dot(inner, down[...], preferred_element_type=f32).astype(bf16)
-        partial[g] = share.reshape(2 * Y_RING, block, width)
-        for k in (2, 1, 3, 0):
-            core_copy(g, k).start()
+        for i, n in enumerate(slots):
+            partial[g, n] = share[i * block : (i + 1) * block]
+            if n % 2:
+                core_copy(g, n // 2).start()
 
     def both_cores(g, k, cols):
         return partial[g, 2 * k, :, cols].astype(f32) + from_core[g, k, :, cols].astype(f32)
@@ -601,31 +604,31 @@
     for c in weights[2:]:
         c.wait()
     close_gather(0)
-    multiply(0)
     pass_on(2)
     send_halves(0)
     close_gather(1)
-    multiply(1)
     send_sides(0)
     send_halves(1)
     close_gather(2)
-    multiply(2)
     give_back(0)
     send_sides(1)
     send_halves(2)
     give_back(1)
     send_sides(2)
     give_back(2)
+    picked = [jnp.zeros((local_rows, width), f32) for c in range(top_count)]
     for g in range(capacity):
         for dz, dx in others:
             return_copy(g, -dz % Z_RING, -dx % X_RING).wait_recv()
-    from_tiles(returned, 0, experts * capacity, words, returned_rows)
+        from_tiles(returned, g * experts, experts, words, returned_rows)
+        for c in range(top_count):
+            picked[c] = picked[c] + lax.dot_general(
+                picks[c, pl.ds(g * experts, experts)], returned_rows[...],
+                (((0,), (0,)), ((), ())), preferred_element_type=f32,
+            )
     routed = jnp.zeros((local_rows, width), f32)
     for c in range(top_count):
-        picked = lax.dot_general(
-            picks[c], returned_rows[...], (((0,), (0,)), ((), ())), preferred_element_type=f32
-        )
-        routed = routed + scales[c, :, 0:1] * picked
+        routed = routed + scales[c, :, 0:1] * picked[c]
     out[...] = layer_norm(
         residual_scale * hidden[...].astype(f32) + routed, norm2_gain[...]
     ).astype(bf16)
@@ -727,7 +730,7 @@
             pltpu.VMEM((capacity, 2, block, width), bf16),
             pltpu.VMEM((count, tall, LANES), bf16),
             pltpu.VMEM((count, tall, LANES), bf16),
-            pltpu.VMEM((count, width), bf16),
+            pltpu.VMEM((experts, width), bf16),
             dma((6,)),
             dma((X_RING,)),
             dma((X_RING,)),

time: 116 us -> 115 us (level)
  no operation moved by 1% of the time
where the time goes in v6:
time: 115 us
  Pallas kernels  112 us (97%)
  local copies, waits for them, and re-layouts  1.59 us (1%)
  between operations  1.31 us (1%)
    pallas_call x1, Pallas kernels, on_device(): pl.pallas_call(functools.partial(layer_kernel, tok, capacity), out_shape=...  112 us

profile of v6, /device:TPU:2, one launch (start us, length us, event | category | flops | bytes accessed | tf_op | source)
XLA Modules:
  0.0 115.0 jit_solution(1441974471455076195)
XLA Ops:
  1.3 112.1 %layer.1 = bf16[40,2048]{1,0:T(8,128)(2,1)} custom-call(bf16[40,2048]{1,0:T(8,128)(2,1)} %residual.1, bf16[320,128]{1,0:T(8,128)(2,1)} %query_narrow.1, bf16[320,128]{1,0:T(8,128)(2,1)} %key_narrow.1, bf16[320,128]{1,0:T(8,128)(2,1)} %value_narrow.1, bf16[320,256]{1,0:T(8,128)(2,1)} %query_wide.1, bf16[320,256]{1,0:T(8,128)(2,1)} %key_wide.1, ...), custom_call_target="tpu_custom_call" | custom-call | tf_op jit(solution)/shard_map/layer/pallas_call | solution.py:696
  113.4 1.6 %copy.23 = bf16[40,2048]{1,0:T(8,128)(2,1)} copy(bf16[40,2048]{1,0:T(8,128)(2,1)} %layer.1) | data formatting | bytes 327680
